TPU v7x, 32 devices: a whole 2x2x4 slice. The times are simulated.
32 devices in a mesh: ep: 16 (over z, y, x), tp: 2 (over core).
Axes of the slice: x: 2, y: 2, z: 4, core: 2. Of those that a mesh axis runs over, the one named last changes fastest.
Arguments:
- tokens: bfloat16 [2048, 2048], P('ep'), may hold values from -6 to 6
- cotangent: bfloat16 [2048, 2048], P('ep'), may hold values from -0.625 to 0.625
- routes: int32 [2048, 2], P('ep'), may hold values from 0 to 15, as said below
- router_group: bfloat16 [2048, 4], replicated, may hold values from -0.125 to 0.125
- router_expert: bfloat16 [2048, 16], replicated, may hold values from -0.125 to 0.125
- gate_proj: bfloat16 [16, 2048, 512], P('ep', None, 'tp'), may hold values from -0.125 to 0.125
- up_proj: bfloat16 [16, 2048, 512], P('ep', None, 'tp'), may hold values from -0.125 to 0.125
- down_proj: bfloat16 [16, 512, 2048], P('ep', 'tp'), may hold values from -0.25 to 0.25
Outputs:
- token_grad: bfloat16 [2048, 2048], P('ep', 'tp')
- gate_grad: bfloat16 [16, 2048, 512], P('ep', None, 'tp')
- up_grad: bfloat16 [16, 2048, 512], P('ep', None, 'tp')
- down_grad: bfloat16 [16, 512, 2048], P('ep', 'tp')
- gate_rows: float32 [16, 2048], P('ep')
- up_rows: float32 [16, 2048], P('ep')
- down_rows: float32 [16, 512], P('ep', 'tp')
- router_expert_grad: float32 [2048, 16], P(('ep', 'tp'))
- router_group_grad: float32 [2048, 4], P(('ep', 'tp'))
- router_rows: float32 [2048], P(('ep', 'tp'))
Inputs may be any that keep to these rules, and one draw needn't show every extreme that they name: `routes`: the 2 entries of a row are different experts of one group: their quotients by 4 are equal. Among the rows of one device no expert is named more than 32 times, and the experts of one group, the same for all devices, are each named exactly 32 times by the rows of every device.
All inputs are finite; a program needn't handle non-finite values.
Results may differ from a plain program's by a relative error of at most 0.014.
Values may be sent and summed in bfloat16 or wider, within the bound.
No kernel may reach another device: no remote copies, remote signals or barrier semaphores. Data moves between devices by JAX's collectives and lax.ppermute only.
A program may use at most 64 MiB of HBM per device.

v0:
```python
import jax
import jax.numpy as jnp
from jax import lax
from jax.sharding import PartitionSpec as P


def contract_rows(left_side, right_side):
    return lax.dot_general(
        left_side, right_side, (((0,), (0,)), ((), ())), preferred_element_type=jnp.float32
    )


def contract_cols(left_side, right_side):
    return lax.dot_general(
        left_side, right_side, (((1,), (1,)), ((), ())), preferred_element_type=jnp.float32
    )


def router_forward(tokens, routes, router_group, router_expert):
    groups = router_group.shape[1]
    experts = router_expert.shape[1]
    group_logits = jnp.dot(tokens, router_group, preferred_element_type=jnp.float32)
    expert_logits = jnp.dot(tokens, router_expert, preferred_element_type=jnp.float32)
    group_exp = jnp.exp(group_logits)
    group_prob = group_exp / jnp.sum(group_exp, axis=1, keepdims=True)
    chosen_group = routes[:, 0] // (experts // groups)
    group_onehot = (chosen_group[:, None] == jnp.arange(groups, dtype=jnp.int32)[None, :]).astype(
        jnp.float32
    )
    picked = jnp.sum(group_prob * group_onehot, axis=1)
    chosen_logits = jnp.take_along_axis(expert_logits, routes, axis=1)
    paired_exp = jnp.exp(chosen_logits)
    paired = paired_exp / jnp.sum(paired_exp, axis=1, keepdims=True)
    return (group_prob, group_onehot, picked, paired)


def body(tokens, cotangent, routes, router_group, router_expert, gate_proj, up_proj, down_proj):
    tok_rows, model_width = tokens.shape
    top_count = routes.shape[1]
    groups = router_group.shape[1]
    experts = router_expert.shape[1]
    group_width = experts // groups
    capacity = tok_rows // group_width
    tp_count = lax.axis_size("tp")
    tp_index = lax.axis_index("tp")
    col_width = model_width // tp_count
    group_prob, group_onehot, picked, paired = router_forward(
        tokens, routes, router_group, router_expert
    )
    weights = (picked[:, None] * paired).astype(jnp.bfloat16)
    assigned = tok_rows * top_count
    flat_ids = routes.reshape(assigned)
    expert_onehot = (flat_ids[:, None] == jnp.arange(experts, dtype=jnp.int32)[None, :]).astype(
        jnp.int32
    )
    earlier = lax.cumsum(expert_onehot, axis=0) - expert_onehot
    ranking = jnp.sum(earlier * expert_onehot, axis=1)
    slot_index = flat_ids * capacity + ranking
    owners = (
        jnp.full((experts * capacity,), assigned, jnp.int32)
        .at[slot_index]
        .set(jnp.arange(assigned, dtype=jnp.int32))
    )
    source_rows = owners // top_count
    send_tokens = jnp.take(tokens, source_rows, axis=0, mode="fill", fill_value=0)
    send_cot = jnp.take(cotangent, source_rows, axis=0, mode="fill", fill_value=0)
    send_weight = jnp.take(weights.reshape(assigned), owners, axis=0, mode="fill", fill_value=0)
    col_start = tp_index * col_width
    part_tok = lax.dynamic_slice_in_dim(send_tokens, col_start, col_width, 1)
    part_cot = lax.dynamic_slice_in_dim(send_cot, col_start, col_width, 1)
    part_tok, part_cot, got_weight = (
        lax.all_to_all(part_tok, "ep", split_axis=0, concat_axis=0, tiled=True),
        lax.all_to_all(part_cot, "ep", split_axis=0, concat_axis=0, tiled=True),
        lax.all_to_all(send_weight, "ep", split_axis=0, concat_axis=0, tiled=True),
    )
    inputs, upstream = (
        lax.all_gather(part_tok, "tp", axis=1, tiled=True),
        lax.all_gather(part_cot, "tp", axis=1, tiled=True),
    )
    slot_scale = got_weight.astype(jnp.float32)
    gate_mat = gate_proj[0]
    up_mat = up_proj[0]
    down_mat = down_proj[0]
    gate_pre = jnp.dot(inputs, gate_mat, preferred_element_type=jnp.float32)
    up_pre = jnp.dot(inputs, up_mat, preferred_element_type=jnp.float32)
    sigmoid_gate = jax.nn.sigmoid(gate_pre)
    hidden = (gate_pre * sigmoid_gate * up_pre).astype(jnp.bfloat16)
    pulled = contract_cols(upstream, down_mat)
    weight_part = jnp.sum(pulled * hidden.astype(jnp.float32), axis=1)
    dhidden = slot_scale[:, None] * pulled
    gate_delta = (dhidden * up_pre * sigmoid_gate * (1.0 + gate_pre * (1.0 - sigmoid_gate))).astype(
        jnp.bfloat16
    )
    up_delta = (dhidden * gate_pre * sigmoid_gate).astype(jnp.bfloat16)
    scaled_cot = (slot_scale[:, None] * upstream.astype(jnp.float32)).astype(jnp.bfloat16)
    gate_total = contract_rows(inputs, gate_delta)
    up_total = contract_rows(inputs, up_delta)
    down_total = contract_rows(hidden, scaled_cot)
    token_term = contract_cols(gate_delta, gate_mat) + contract_cols(up_delta, up_mat)
    token_sum = lax.psum_scatter(
        token_term.astype(jnp.bfloat16), "tp", scatter_dimension=1, tiled=True
    )
    weight_sum, gate_sq, up_sq = lax.psum(
        (
            weight_part,
            jnp.sum(gate_total * gate_total, axis=1),
            jnp.sum(up_total * up_total, axis=1),
        ),
        "tp",
    )
    returned, weight_back = (
        lax.all_to_all(token_sum, "ep", split_axis=0, concat_axis=0, tiled=True),
        lax.all_to_all(
            weight_sum.astype(jnp.bfloat16), "ep", split_axis=0, concat_axis=0, tiled=True
        ),
    )
    back_rows = jnp.take(returned, slot_index, axis=0)
    expert_part = jnp.sum(
        back_rows.reshape(tok_rows, top_count, col_width).astype(jnp.float32), axis=1
    )
    dweight = jnp.take(weight_back, slot_index, axis=0).astype(jnp.float32)
    dweight = dweight.reshape(tok_rows, top_count)
    dpicked = jnp.sum(dweight * paired, axis=1)
    dpaired = dweight * picked[:, None]
    dchosen = paired * (dpaired - jnp.sum(paired * dpaired, axis=1, keepdims=True))
    dgroup = ((dpicked * picked)[:, None] * (group_onehot - group_prob)).astype(jnp.bfloat16)
    route_onehot = (
        routes[:, :, None] == jnp.arange(experts, dtype=jnp.int32)[None, None, :]
    ).astype(jnp.float32)
    dexpert = jnp.sum(dchosen[:, :, None] * route_onehot, axis=1).astype(jnp.bfloat16)
    own_cols = tp_index * col_width
    group_cols = lax.dynamic_slice_in_dim(router_group, own_cols, col_width, 0)
    expert_cols = lax.dynamic_slice_in_dim(router_expert, own_cols, col_width, 0)
    router_part = contract_cols(dgroup, group_cols) + contract_cols(dexpert, expert_cols)
    token_grad = (expert_part + router_part).astype(jnp.bfloat16)
    row_count = tok_rows // tp_count
    row_start = tp_index * row_count
    own_tokens = lax.dynamic_slice_in_dim(tokens, row_start, row_count, 0)
    expert_term = contract_rows(
        own_tokens, lax.dynamic_slice_in_dim(dexpert, row_start, row_count, 0)
    )
    group_term = contract_rows(
        own_tokens, lax.dynamic_slice_in_dim(dgroup, row_start, row_count, 0)
    )
    router_expert_grad, router_group_grad = (
        lax.psum_scatter(expert_term, ("ep", "tp"), scatter_dimension=0, tiled=True),
        lax.psum_scatter(group_term, ("ep", "tp"), scatter_dimension=0, tiled=True),
    )
    router_rows = jnp.sum(router_expert_grad * router_expert_grad, axis=1) + jnp.sum(
        router_group_grad * router_group_grad, axis=1
    )
    down_sq = jnp.sum(down_total * down_total, axis=1)
    return (
        token_grad,
        gate_total.astype(jnp.bfloat16)[None],
        up_total.astype(jnp.bfloat16)[None],
        down_total.astype(jnp.bfloat16)[None],
        gate_sq[None],
        up_sq[None],
        down_sq[None],
        router_expert_grad,
        router_group_grad,
        router_rows,
    )


def solution(mesh):
    return jax.shard_map(
        body,
        mesh=mesh,
        in_specs=(
            P("ep", None),
            P("ep", None),
            P("ep", None),
            P(),
            P(),
            P("ep", None, "tp"),
            P("ep", None, "tp"),
            P("ep", "tp", None),
        ),
        out_specs=(
            P("ep", "tp"),
            P("ep", None, "tp"),
            P("ep", None, "tp"),
            P("ep", "tp", None),
            P("ep", None),
            P("ep", None),
            P("ep", "tp"),
            P(("ep", "tp"), None),
            P(("ep", "tp"), None),
            P(("ep", "tp")),
        ),
        check_vma=False,
    )
```

profile of v0, /device:TPU:0, one launch (start us, length us, event | category | flops | bytes accessed | tf_op | source)
XLA Modules:
  0.0 438.0 jit_solution(13447635716263064559)
XLA Ops:
  11.7 6.4 %gather_fusion.5 = bf16[512,2048]{1,0:T(8,128)(2,1)} fusion(bf16[128,2048]{1,0:T(8,128)(2,1)} %param.10, s32[1024]{0:T(1024)S(1)} %pad_clamp_fusion.1), kind=kCustom, calls=%fused_computation.1.clone | custom fusion | bytes 4196352 | tf_op jit(solution)/shard_map/jit(_take)/gather | solution.py:65
  18.1 3.3 gather_fusion.4
  21.5 2.9 dynamic-slice_select_fusion.1
  24.4 34.6 %all_to_all.55 = bf16[16,32,1024]{2,1,0:T(8,128)(2,1)} all-to-all(bf16[16,32,1024]{2,1,0:T(8,128)(2,1)S(1)} %bitcast.77), channel_id=1, replica_groups=mesh['ep'=16,'tp'=2] {'ep'}, dimensions={0} | all-to-all | bytes 2097152 | tf_op jit(solution)/shard_map/all_to_all | solution.py:72
  59.0 4.1 all-to-all-start.1
  63.7 23.1 %all-to-all-done.1 = bf16[16,32,1024]{2,1,0:T(8,128)(2,1)S(1)} async-done(((bf16[16,32,1024]{2,1,0:T(8,128)(2,1)}), bf16[16,32,1024]{2,1,0:T(8,128)(2,1)S(1)}, u32[]{:S(2)}, u32[]{:S(2)}) %all-to-all-start.1) | async-done | bytes 1048608 | tf_op jit(solution)/shard_map/all_to_all | solution.py:73
  88.1 2.0 gather_fusion.3
  90.7 3.4 gather_fusion
  94.2 13.1 %all_to_all.56 = bf16[16,32,1]{1,2,0:T(2,128)(2,1)S(1)} all-to-all(bf16[16,32,1]{1,2,0:T(2,128)(2,1)S(1)} %select_n.106), channel_id=1, replica_groups=mesh['ep'=16,'tp'=2] {'ep'}, dimensions={0} | all-to-all | bytes 2048 | tf_op jit(solution)/shard_map/all_to_all | solution.py:74
  107.4 3.3 fusion.6
  110.7 1.6 fusion.9
  112.2 3.1 multiply_reduce_fusion.3
  116.1 2.2 add_convert_fusion
  118.3 3.4 convert_bitcast_fusion.2
  121.7 1.7 convert_bitcast_fusion.1
  123.4 4.0 all-reduce
  127.5 9.9 %all_to_all.57 = bf16[16,32,1]{1,2,0:T(2,128)(2,1)S(1)} all-to-all(bf16[16,32,1]{1,2,0:T(2,128)(2,1)S(1)} %all_to_all.49), channel_id=1, replica_groups=mesh['ep'=16,'tp'=2] {'ep'}, dimensions={0} | all-to-all | bytes 2048 | tf_op jit(solution)/shard_map/all_to_all | solution.py:113
  137.4 3.7 all-to-all-start.3
  141.3 2.3 copy.76
  143.6 2.3 copy.75
  145.8 4.0 multiply_reduce_fusion
  149.9 1.9 gather_fusion.2
  155.4 136.2 %reduce-scatter.12.cloned.1.call-done = f32[64,4]{1,0:T(8,128)} async-done(((f32[2048,4]{1,0:T(8,128)}), f32[64,4]{1,0:T(8,128)}) %reduce-scatter.12.cloned.1.call-update) | async-done | bytes 1040
  292.5 133.8 %reduce-scatter.10.cloned.1.call-done = f32[64,16]{1,0:T(8,128)} async-done(((f32[2048,16]{1,0:T(8,128)}), f32[64,16]{1,0:T(8,128)}) %reduce-scatter.10.cloned.1.call-update) | async-done | bytes 4112
  (101 shorter events, 17.9 us)
Async XLA Ops:
  7.2 100.2 %copy-start = (bf16[1,2048,256]{2,1,0:T(8,128)(2,1)S(1)}, bf16[1,2048,256]{2,1,0:T(8,128)(2,1)}, u32[]{:S(2)}) copy-start(bf16[1,2048,256]{2,1,0:T(8,128)(2,1)} %param.15) | copy-start | bytes 3145732
  7.2 100.2 %all-gather.5.cloned.1.call-start = ((), (), s32[]{:S(2)}) async-start(), calls=%async_computation.9 | async-start | bytes 3145728 | tf_op jit(solution)/shard_map/all_gather | solution.py:77
  11.7 6.4 %copy-start.2 = (bf16[128,2048]{1,0:T(8,128)(2,1)S(1)}, bf16[128,2048]{1,0:T(8,128)(2,1)}, u32[]{:S(2)}) copy-start(bf16[128,2048]{1,0:T(8,128)(2,1)} %param.11) | copy-start | bytes 1572868
  58.9 4.2 copy-start.1
  58.9 4.2 copy-start.6
  58.9 4.5 %copy-start.5 = (bf16[2048,16]{0,1:T(8,128)(2,1)S(1)}, bf16[2048,16]{0,1:T(8,128)(2,1)}, u32[]{:S(2)}) copy-start(bf16[2048,16]{0,1:T(8,128)(2,1)} %param.14) | copy-start | bytes 196612
  59.0 28.8 %copy-start.7 = (s32[128,2]{0,1:T(2,128)S(1)}, s32[128,2]{0,1:T(2,128)}, u32[]{:S(2)}) copy-start(s32[128,2]{0,1:T(2,128)} %param.12) | copy-start | bytes 3076
  59.0 27.8 %all-to-all-start.1 = ((bf16[16,32,1024]{2,1,0:T(8,128)(2,1)}), bf16[16,32,1024]{2,1,0:T(8,128)(2,1)S(1)}, u32[]{:S(2)}, u32[]{:S(2)}) async-start(bf16[16,32,1024]{2,1,0:T(8,128)(2,1)} %bitcast.5), calls=%async_computation.1 | async-start | bytes 2097152 | tf_op jit(solution)/shard_map/all_to_all | solution.py:73
  63.1 49.1 %all-gather.3.cloned.1.call-start = ((), (), s32[]{:S(2)}) async-start(), calls=%async_computation.8 | async-start | bytes 3145728 | tf_op jit(solution)/shard_map/all_gather | solution.py:78
  86.8 1.0 copy-start.3
  87.7 49.6 %reduce-scatter.8.cloned.1.call-start = ((), (), s32[]{:S(2)}) async-start(), calls=%async_computation.10 | async-start | bytes 3145728 | tf_op jit(solution)/shard_map/reduce_scatter | solution.py:100
  94.0 16.6 %copy-start.4 = (bf16[1,2048,256]{2,1,0:T(8,128)(2,1)S(1)}, bf16[1,2048,256]{2,1,0:T(8,128)(2,1)}, u32[]{:S(2)}) copy-start(bf16[1,2048,256]{2,1,0:T(8,128)(2,1)} %param.16) | copy-start | bytes 3145732
  107.4 3.3 copy-start.10
  118.3 3.4 copy-start.11
  137.4 290.3 %all-to-all-start.3 = ((bf16[16,32,1024]{2,1,0:T(8,128)(2,1)}), bf16[16,32,1024]{2,1,0:T(8,128)(2,1)S(1)}, u32[]{:S(2)}, u32[]{:S(2)}) async-start(bf16[16,32,1024]{2,1,0:T(8,128)(2,1)} %bitcast.80), calls=%async_computation.4 | async-start | bytes 2097152 | tf_op jit(solution)/shard_map/all_to_all | solution.py:112
  141.0 150.6 %reduce-scatter.12.cloned.1.call-start = ((), (), s32[]{:S(2)}) async-start(), calls=%async_computation.12 | async-start | bytes 1081344
  153.6 272.7 %reduce-scatter.10.cloned.1.call-start = ((), (), s32[]{:S(2)}) async-start(), calls=%async_computation.11 | async-start | bytes 1081344
  292.4 136.3 %copy-start.9 = (f32[64,4]{0,1:T(4,128)}, f32[64,4]{0,1:T(4,128)S(1)}, u32[]{:S(2)}) copy-start(f32[64,4]{0,1:T(4,128)S(1)} %copy.80) | copy-start | bytes 3076
  427.1 1.7 copy-start.8
Sparse Core Ops, SparseCore 0:
  59.1 8.8 all-gather.4
  87.9 10.8 all-gather.2
  118.4 5.9 reduce-scatter.7
  153.7 137.8 reduce-scatter.11
  293.7 132.4 reduce-scatter.9
where the time goes:
time: 439 us; the launch traced here: 438 us
  waiting for transfers between devices  293 us (67%)
  blocking collectives  61.5 us (14%)
  local copies, waits for them, and re-layouts  30.1 us (7%)
  matrix products  24.5 us (6%)
  between operations  14.1 us (3%)
  starting transfers between devices  7.95 us (2%)
  other arithmetic  6.71 us (2%)
    unnamed x7, waiting for transfers between devices  270 us
    all_to_all x1, blocking collectives, body(): lax.all_to_all(part_tok, 'ep', split_axis=0, concat_axis=0, tiled=True)  34.6 us
    all_to_all x1, waiting for transfers between devices, body(): lax.all_to_all(part_cot, 'ep', split_axis=0, concat_axis=0, tiled=True)  23.1 us
    all_to_all x1, blocking collectives, body(): lax.all_to_all(send_weight, 'ep', split_axis=0, concat_axis=0, tiled=True)  13.1 us
    all_to_all x1, blocking collectives, body(): lax.all_to_all(weight_sum.astype(jnp.bfloat16), 'ep', split_axis=0, conca...  9.87 us
    dot_general x3, matrix products, contract_rows(): lax.dot_general(left_side, right_side, (((0,), (0,)), ((), ())), preferre...  9.08 us
  transfers between devices with their start and end apart: 7, of which 3 were waited for; matrix products, arithmetic and copies ran while one was open for 8% of the time, Pallas kernels for 0%

commit v1 on v0

v1 whole, which is shorter than its diff:
```python
import functools

import jax
import jax.numpy as jnp
from jax import lax
from jax.experimental import pallas as pl
from jax.experimental.pallas import tpu as pltpu
from jax.sharding import PartitionSpec as P


BF = jnp.bfloat16
F32 = jnp.float32


def dot(a, b):
    return jnp.dot(a, b, preferred_element_type=F32)


def dot_nt(a, b):
    return lax.dot_general(a, b, (((1,), (1,)), ((), ())), preferred_element_type=F32)


def dot_tn(a, b):
    return lax.dot_general(a, b, (((0,), (0,)), ((), ())), preferred_element_type=F32)


def iota(shape, axis):
    return lax.broadcasted_iota(jnp.int32, shape, axis)


def onehot(mask):
    return jnp.where(mask, 1.0, 0.0).astype(BF)


def call(kernel, out_shapes, args, scratch=(), flops=0, in_hbm=(), limit=24 * 2**20):
    vmem = pl.BlockSpec(memory_space=pltpu.VMEM)
    smem = pl.BlockSpec(memory_space=pltpu.SMEM)
    hbm = pl.BlockSpec(memory_space=pltpu.HBM)
    in_specs = [
        smem if a.ndim == 1 and a.dtype == jnp.int32 else hbm if i in in_hbm else vmem
        for i, a in enumerate(args)
    ]
    return pl.pallas_call(
        kernel,
        out_shape=out_shapes,
        in_specs=in_specs,
        out_specs=jax.tree.map(lambda _: vmem, out_shapes),
        scratch_shapes=list(scratch),
        cost_estimate=pl.CostEstimate(flops=flops, bytes_accessed=0, transcendentals=0),
        compiler_params=pltpu.CompilerParams(vmem_limit_bytes=limit),
    )(*args)


def group_onehots(rank_row, group_row, my_group, groups, slots):
    toks = rank_row.shape[1]
    row = iota((slots, toks), 0).astype(F32)
    hit = row == rank_row
    outs = []
    for k in range(groups):
        other = jnp.bitwise_xor(my_group, k).astype(F32)
        outs.append(onehot(jnp.logical_and(hit, group_row == other)))
    return outs


def slot_hits(shape, member, cap, per, s0, s1, slot_axis):
    slot = iota(shape, slot_axis)
    block = slot // per
    want = (jnp.bitwise_xor(member, block) * cap + slot % cap + 1).astype(F32)
    return s0 == want, s1 == want


def prep_kernel(dims, ids, tok_hbm, cot_hbm, routes_hbm, rg_hbm, re_hbm, *rest):
    groups, width, cap, slots, half = dims
    outs, (tok_ref, cot_ref, routes_ref, rg_ref, re_ref, sems) = rest[:-6], rest[-6:]
    z_tok, z_cot = outs[:groups], outs[groups : 2 * groups - 1]
    own, stat_ref = outs[2 * groups - 1 : -1], outs[-1]
    toks, _ = tok_ref.shape
    experts = re_ref.shape[0]
    my_group, my_member = ids[0], ids[1]
    start = pl.multiple_of(ids[2], 128)
    copies = [
        pltpu.make_async_copy(src, dst, sems.at[i])
        for i, (src, dst) in enumerate(
            (
                (routes_hbm, routes_ref),
                (re_hbm, re_ref),
                (rg_hbm, rg_ref),
                (tok_hbm, tok_ref),
                (cot_hbm.at[:, pl.ds(start, half)], cot_ref),
            )
        )
    ]
    for copy in copies:
        copy.start()
    earlier = onehot(iota((toks, toks), 0) < iota((toks, toks), 1))
    for copy in copies[:4]:
        copy.wait()
    tokens = tok_ref[...]
    e_t = dot_nt(re_ref[...], tokens)
    g_t = dot_nt(rg_ref[...], tokens)
    g_t = jnp.concatenate([g_t, jnp.zeros((8 - groups, toks), F32)], axis=0)
    routes = routes_ref[...].astype(F32)
    r0, r1 = routes[0:1], routes[1:2]
    grow = iota((8, toks), 0)
    gexp = jnp.where(grow < groups, jnp.exp(g_t), 0.0)
    gprob = gexp / jnp.sum(gexp, axis=0, keepdims=True)
    low = (grow * width).astype(F32)
    gmask = jnp.logical_and(r0 >= low, r0 < low + width)
    picked = jnp.sum(jnp.where(gmask, gprob, 0.0), axis=0, keepdims=True)
    group_row = jnp.sum(jnp.where(gmask, grow.astype(F32), 0.0), axis=0, keepdims=True)
    erow = iota((experts, toks), 0).astype(F32)
    a0, a1 = erow == r0, erow == r1
    eexp = jnp.exp(e_t)
    x0 = jnp.sum(jnp.where(a0, eexp, 0.0), axis=0, keepdims=True)
    x1 = jnp.sum(jnp.where(a1, eexp, 0.0), axis=0, keepdims=True)
    p0, p1 = x0 / (x0 + x1), x1 / (x0 + x1)
    cum = dot(onehot(jnp.logical_or(a0, a1)), earlier)
    rank0 = jnp.sum(jnp.where(a0, cum, 0.0), axis=0, keepdims=True)
    rank1 = jnp.sum(jnp.where(a1, cum, 0.0), axis=0, keepdims=True)
    gcum = dot(onehot(gmask), earlier)
    rank_g = jnp.sum(jnp.where(gmask, gcum, 0.0), axis=0, keepdims=True)
    base = group_row * width
    s0 = (r0 - base) * cap + rank0 + 1.0
    s1 = (r1 - base) * cap + rank1 + 1.0
    mrow = iota((128, toks), 0)
    meta = jnp.where(mrow == 0, picked * p0, 0.0)
    meta = jnp.where(mrow == 1, picked * p1, meta)
    meta = jnp.where(mrow == 2, s0, meta)
    meta = jnp.where(mrow == 3, s1, meta)
    for i, v in enumerate([picked, p0, p1] + [gprob[j : j + 1] for j in range(groups)]):
        top = v.astype(BF).astype(F32)
        meta = jnp.where(mrow == 4 + 2 * i, top, meta)
        meta = jnp.where(mrow == 5 + 2 * i, v - top, meta)
    meta = meta.astype(BF)
    stat_ref[...] = jnp.where(iota((8, toks), 0) == 0, rank_g, group_row)
    sel = group_onehots(rank_g, group_row, my_group, groups, slots)
    mine = group_row == my_group.astype(F32)
    hit0, hit1 = slot_hits(
        (width * cap, toks), my_member, cap, cap,
        jnp.where(mine, s0, 0.0), jnp.where(mine, s1, 0.0), 0,
    )
    spread = onehot(jnp.logical_or(hit0, hit1))
    weight = dot_nt(onehot(hit0), meta)[:, 0:1] + dot_nt(onehot(hit1), meta)[:, 1:2]
    every = jnp.concatenate(sel + [spread], axis=0)
    metas = dot_nt(jnp.concatenate(sel, axis=0), meta).astype(BF)
    first = groups * slots
    moved_tok = dot(every, tok_ref[:, pl.ds(start, half)]).astype(BF)
    for k in range(groups):
        z_tok[k][:, :half] = moved_tok[k * slots : (k + 1) * slots]
        z_tok[k][:, half:] = metas[k * slots : (k + 1) * slots]
    copies[4].wait()
    moved_cot = dot(every[slots:], cot_ref[...]).astype(BF)
    for k in range(1, groups):
        z_cot[k - 1][...] = moved_cot[(k - 1) * slots : k * slots]
    wide = jnp.broadcast_to(weight, (width * cap, 128)).astype(BF)
    for k in range(width):
        at = first + k * cap
        own[k][:, :half] = moved_tok[at : at + cap]
        own[k][:, half : 2 * half] = moved_cot[at - slots : at - slots + cap]
        own[k][:, 2 * half :] = wide[k * cap : (k + 1) * cap]


def spread_kernel(dims, with_weight, ids, *refs):
    groups, width, cap, slots, half = dims
    srcs = groups - 1
    z, outs = refs[: len(refs) - width], refs[len(refs) - width :]
    tok = z[:srcs]
    meta = jnp.concatenate([r[:, half:] for r in tok], axis=0).astype(F32)
    rows = jnp.transpose(meta)
    data = tok if with_weight else z[srcs:]
    data = jnp.concatenate([r[:, :half] for r in data], axis=0)
    shape = (width * srcs * cap, srcs * slots)
    same = iota(shape, 0) // cap % srcs == iota(shape, 1) // slots
    hit0, hit1 = slot_hits(shape, ids[1], cap, srcs * cap, rows[2:3], rows[3:4], 0)
    hit0, hit1 = jnp.logical_and(same, hit0), jnp.logical_and(same, hit1)
    spread = dot(onehot(jnp.logical_or(hit0, hit1)), data).astype(BF)
    per = srcs * cap
    if with_weight:
        meta = meta.astype(BF)
        weight = dot(onehot(hit0), meta)[:, 0:1] + dot(onehot(hit1), meta)[:, 1:2]
        wide = jnp.broadcast_to(weight, (width * per, 128)).astype(BF)
    for k in range(width):
        outs[k][:, :half] = spread[k * per : (k + 1) * per]
        if with_weight:
            outs[k][:, half:] = wide[k * per : (k + 1) * per]


def assemble(ids, own, other, out_ref, half, at):
    mine = pl.multiple_of(ids[2], 128)
    theirs = pl.multiple_of(half - ids[2], 128)
    width = len(own[0])
    rows = out_ref.shape[0] // width
    for base, (first, second) in ((mine, own), (theirs, other)):
        for k in range(width):
            low = first[k].shape[0]
            out_ref[k * rows : k * rows + low, pl.ds(base, half)] = first[k][:, at : at + half]
            out_ref[k * rows + low : (k + 1) * rows, pl.ds(base, half)] = second[k][:, :half]


def forward_kernel(width, half, ids, *refs):
    parts = [refs[i * width : (i + 1) * width] for i in range(4)]
    gate_ref, up_ref, x_ref, gp_ref, upp_ref = refs[4 * width :]
    assemble(ids, parts[:2], parts[2:], x_ref, half, 0)
    x = x_ref[...]
    gp_ref[...] = dot(x, gate_ref[...])
    upp_ref[...] = dot(x, up_ref[...])


def delta_kernel(width, half, ids, *refs):
    parts = [refs[i * width : (i + 1) * width] for i in range(4)]
    tok = refs[4 * width : 5 * width]
    down_ref, gp_ref, upp_ref, gd_ref, ud_ref, hid_ref, c_ref, w_ref, s_ref = refs[5 * width :]
    assemble(ids, parts[:2], parts[2:], c_ref, half, half)
    rows = c_ref.shape[0] // width
    for k in range(width):
        low = parts[0][k].shape[0]
        w_ref[k * rows : k * rows + low, :] = parts[0][k][:, 2 * half :].astype(F32)
        w_ref[k * rows + low : (k + 1) * rows, :] = tok[k][:, half:].astype(F32)
    pulled = dot_nt(c_ref[...], down_ref[...])
    gate_pre, up_pre = gp_ref[...], upp_ref[...]
    sig = 1.0 / (1.0 + jnp.exp(-gate_pre))
    silu = gate_pre * sig
    hidden = (silu * up_pre).astype(BF)
    hid_ref[...] = hidden
    dh = w_ref[:, 0:1] * pulled
    gd_ref[...] = (dh * up_pre * sig * (1.0 + gate_pre * (1.0 - sig))).astype(BF)
    ud_ref[...] = (dh * silu).astype(BF)
    part = jnp.sum(pulled * hidden.astype(F32), axis=1, keepdims=True)
    top = part.astype(BF).astype(F32)
    lane = iota((part.shape[0], 128), 1)
    s_ref[...] = jnp.where(lane == 0, top, jnp.where(lane == 1, part - top, 0.0)).astype(BF)


def term_kernel(own, width, half, ids, gd_ref, ud_ref, gate_ref, up_ref, s_ref, *outs):
    base = ids[2] if own else half - ids[2]
    rows = outs[0].shape[0]
    gd, ud = gd_ref[...], ud_ref[...]
    step = 256
    for k in range(width):
        outs[k][:, half:] = s_ref[k * rows : (k + 1) * rows, :]

    @pl.loop(0, half // step)
    def _(i):
        at = pl.ds(pl.multiple_of(base + i * step, step), step)
        term = dot_nt(gd, gate_ref[at, :]) + dot_nt(ud, up_ref[at, :])
        to = pl.ds(pl.multiple_of(i * step, step), step)
        for k in range(width):
            outs[k][:, to] = term[k * rows : (k + 1) * rows].astype(BF)


def add_kernel(width, half, *refs):
    for k in range(width):
        total = refs[k][...].astype(F32) + refs[width + k][...].astype(F32)
        out = refs[2 * width + k]
        out[:, :half] = total[:, :half].astype(BF)
        tail = total[:, half : half + 1] + total[:, half + 1 : half + 2]
        out[:, half:] = jnp.broadcast_to(tail, (total.shape[0], 128)).astype(BF)


def grad_kernel(x_ref, gd_ref, ud_ref, gg_ref, ug_ref, gsq_ref, usq_ref):
    step = 256

    @pl.loop(0, x_ref.shape[1] // step)
    def _(i):
        at = pl.ds(pl.multiple_of(i * step, step), step)
        xt = jnp.transpose(x_ref[:, at])
        for d_ref, out, sq in ((gd_ref, gg_ref, gsq_ref), (ud_ref, ug_ref, usq_ref)):
            total = dot(xt, d_ref[...])
            out[at, :] = total.astype(BF)
            part = jnp.sum(total * total, axis=1, keepdims=True)
            sq[:, at] = jnp.transpose(jnp.broadcast_to(part, (step, 128)))[:1]


def down_kernel(c_ref, w_ref, hid_ref, out_ref, sq_ref, acc, hid_t):
    step = 256
    acc[...] = jnp.zeros_like(acc)
    hid_t[...] = jnp.transpose(hid_ref[...])

    @pl.loop(0, c_ref.shape[1] // step)
    def _(i):
        at = pl.ds(pl.multiple_of(i * step, step), step)
        scaled = (w_ref[:, 0:1] * c_ref[:, at].astype(F32)).astype(BF)
        total = dot(hid_t[...], scaled)
        out_ref[:, at] = total.astype(BF)
        acc[...] += jnp.sum(total * total, axis=1, keepdims=True)

    sq_ref[...] = jnp.transpose(jnp.broadcast_to(acc[...], (acc.shape[0], 128)))[:1]


def reduce_kernel(dims, got_ref, e_ref, g_ref, rows_ref):
    experts, groups, own = dims
    total = jnp.sum(got_ref[...], axis=0)
    pack = 128 // own
    total = jnp.concatenate([total[:, i * own : (i + 1) * own] for i in range(pack)], axis=0)
    by_expert, by_group = total[:experts], total[experts : experts + groups]
    e_ref[...] = by_expert
    g_ref[...] = by_group
    rows_ref[...] = jnp.sum(by_expert * by_expert, axis=0, keepdims=True) + jnp.sum(
        by_group * by_group, axis=0, keepdims=True
    )


def merge_kernel(dims, experts, ids, rt_ref, *refs):
    groups, width, cap, slots, half = dims
    blocks, tok = refs[:width], refs[width : width + groups]
    outs, (mine_ref, other_ref) = refs[width + groups : -2], refs[-2:]
    start = pl.multiple_of(ids[2], 128)
    meta = jnp.concatenate([r[:, half:] for r in tok], axis=0).astype(F32)
    shape = (groups * slots, width * groups * cap)
    same = iota(shape, 1) // cap % groups == iota(shape, 0) // slots
    hit0, hit1 = slot_hits(shape, ids[1], cap, groups * cap, meta[:, 2:3], meta[:, 3:4], 1)
    hit0, hit1 = jnp.logical_and(same, hit0), jnp.logical_and(same, hit1)
    sent = jnp.concatenate([r[:, half:] for r in blocks], axis=0)
    lane = iota(meta.shape, 1)
    meta = jnp.where(lane == 126, dot(onehot(hit0), sent), meta)
    meta = jnp.where(lane == 127, dot(onehot(hit1), sent), meta)
    rows = jnp.transpose(meta)
    picked, p0, p1 = [rows[4 + 2 * i : 5 + 2 * i] + rows[5 + 2 * i : 6 + 2 * i] for i in range(3)]
    s0, s1 = rows[126:127], rows[127:128]
    dpicked = s0 * p0 + s1 * p1
    q0, q1 = picked * s0, picked * s1
    mean = p0 * q0 + p1 * q1
    c0, c1 = p0 * (q0 - mean), p1 * (q1 - mean)
    toks = groups * slots
    grow = iota((8, toks), 0)
    dgroup = jnp.zeros((8, toks), F32)
    for j in range(groups):
        at = 10 + 2 * j
        prob = rows[at : at + 1] + rows[at + 1 : at + 2]
        hot = jnp.where(ids[0] == j, 1.0, 0.0)
        dgroup = jnp.where(grow == j, dpicked * picked * (hot - prob), dgroup)
    low = ids[0] * width
    erow = ((iota((experts, toks), 0) - low) * cap).astype(F32)
    dexpert = jnp.zeros((experts, toks), F32)
    for c, slot in ((c0, rows[2:3]), (c1, rows[3:4])):
        inside = jnp.logical_and(slot > erow, slot <= erow + cap)
        dexpert += jnp.where(inside, c, 0.0)
    d = jnp.concatenate([dexpert, dgroup], axis=0).astype(BF)
    hit = onehot(jnp.logical_or(hit0, hit1))
    total = dot(hit, jnp.concatenate([r[:, :half] for r in blocks], axis=0))
    total += dot_tn(d, rt_ref[:, pl.ds(start, half)])
    for j in range(groups):
        outs[j][...] = total[j * slots : (j + 1) * slots].astype(BF)
    part = dot(d, jnp.concatenate([r[:, :half] for r in tok], axis=0))
    count, high = mine_ref.shape[:2]
    own = half // (2 * count)
    pack = 128 // own
    part = jnp.concatenate([part, jnp.zeros((high * pack - part.shape[0], half), F32)], axis=0)
    for j in range(count):
        low, up = part[:, 2 * j * own : (2 * j + 1) * own], part[:, (2 * j + 1) * own : (2 * j + 2) * own]
        for ref, cols in (
            (mine_ref, jnp.where(ids[3] == 0, low, up)),
            (other_ref, jnp.where(ids[3] == 0, up, low)),
        ):
            ref[j] = jnp.concatenate(
                [cols[i * high : (i + 1) * high] for i in range(pack)], axis=1
            )


def final_kernel(dims, ids, stat_ref, *refs):
    groups, slots = dims
    blocks, out_ref = refs[:groups], refs[groups]
    sel = group_onehots(stat_ref[0:1, :], stat_ref[1:2, :], ids[0], groups, slots)
    every = jnp.concatenate(sel, axis=0)
    out_ref[...] = dot_tn(every, jnp.concatenate([r[...] for r in blocks], axis=0)).astype(BF)


def body(tokens, cotangent, routes, router_group, router_expert, gate_proj, up_proj, down_proj):
    toks, model = tokens.shape
    top = routes.shape[1]
    groups = router_group.shape[1]
    experts = router_expert.shape[1]
    width = experts // groups
    cap = toks // width
    slots = width * cap // top
    ep = lax.axis_size("ep")
    tp = lax.axis_size("tp")
    half = model // tp
    hidden = gate_proj.shape[2]
    rows = groups * cap
    total_rows = width * rows
    ep_i, tp_i = lax.axis_index("ep"), lax.axis_index("tp")
    ids = jnp.stack([ep_i // width, ep_i % width, tp_i * half, tp_i]).astype(jnp.int32)
    dims = (groups, width, cap, slots, half)

    def sds(shape, dtype=BF):
        return jax.ShapeDtypeStruct(shape, dtype)

    def over_groups(blocks):
        moved = []
        for k, x in enumerate(blocks, 1):
            perm = [(i, ((i // width) ^ k) * width + i % width) for i in range(ep)]
            moved.append(lax.ppermute(x, "ep", perm))
        return moved

    def over_members(blocks):
        moved = [blocks[0]]
        for k in range(1, width):
            moved.append(lax.ppermute(blocks[k], "ep", [(i, i ^ k) for i in range(ep)]))
        return moved

    def swap(x):
        return lax.ppermute(x, "tp", [(i, tp - 1 - i) for i in range(tp)])

    def swaps(blocks):
        return [swap(x) for x in blocks]

    flat = total_rows * model * hidden
    small = toks * toks * model
    srcs = groups - 1
    prep = call(
        functools.partial(prep_kernel, dims),
        [sds((slots, half + 128))] * groups
        + [sds((slots, half))] * srcs
        + [sds((cap, model + 128))] * width
        + [sds((8, toks), F32)],
        (ids, tokens, cotangent, routes.T, router_group.T, router_expert.T),
        scratch=[
            pltpu.VMEM((toks, model), BF),
            pltpu.VMEM((toks, half), BF),
            pltpu.VMEM((top, toks), jnp.int32),
            pltpu.VMEM((groups, model), BF),
            pltpu.VMEM((experts, model), BF),
            pltpu.SemaphoreType.DMA((5,)),
        ],
        in_hbm=(1, 2, 3, 4, 5),
        limit=60 * 2**20,
        flops=4 * small,
    )
    z_tok, z_cot, near, stat = (
        prep[:groups], prep[groups : groups + srcs], prep[groups + srcs : -1], prep[-1],
    )
    z_own, z_tok = z_tok[0], over_groups(z_tok[1:])
    z_cot = over_groups(z_cot)
    near = over_members(near)
    m_tok = call(
        functools.partial(spread_kernel, dims, True),
        [sds((srcs * cap, half + 128))] * width,
        (ids, *z_tok),
        flops=4 * small,
    )
    m_tok = over_members(m_tok)
    m_cot = call(
        functools.partial(spread_kernel, dims, False),
        [sds((srcs * cap, half))] * width,
        (ids, *z_tok, *z_cot),
        flops=4 * small,
    )
    m_cot = over_members(m_cot)
    o_near = swaps(near)
    o_tok = swaps(m_tok)
    o_cot = swaps(m_cot)
    gate_mat, up_mat, down_mat = gate_proj[0], up_proj[0], down_proj[0]
    x_full, gate_pre, up_pre = call(
        functools.partial(forward_kernel, width, half),
        [
            sds((total_rows, model)),
            sds((total_rows, hidden), F32),
            sds((total_rows, hidden), F32),
        ],
        (ids, *near, *m_tok, *o_near, *o_tok, gate_mat, up_mat),
        flops=4 * flat,
    )
    gate_delta, up_delta, hid, c_full, w_cols, s_part = call(
        functools.partial(delta_kernel, width, half),
        [sds((total_rows, hidden))] * 3
        + [sds((total_rows, model)), sds((total_rows, 128), F32), sds((total_rows, 128))],
        (ids, *near, *m_cot, *o_near, *o_cot, *m_tok, down_mat, gate_pre, up_pre),
        flops=2 * flat,
    )
    terms = []
    for own in (False, True):
        terms.append(
            call(
                functools.partial(term_kernel, own, width, half),
                [sds((rows, half + 128))] * width,
                (ids, gate_delta, up_delta, gate_mat, up_mat, s_part),
                flops=2 * flat,
            )
        )
    back = call(
        functools.partial(add_kernel, width, half),
        [sds((rows, half + 128))] * width,
        (*terms[1], *swaps(terms[0])),
        flops=small,
    )
    back = over_members(back)
    gate_grad, up_grad, gsq, usq = call(
        grad_kernel,
        [sds((model, hidden))] * 2 + [sds((1, model), F32)] * 2,
        (x_full, gate_delta, up_delta),
        flops=4 * flat,
    )
    down_grad, dsq = call(
        down_kernel,
        [sds((hidden, model)), sds((1, hidden), F32)],
        (c_full, w_cols, hid),
        scratch=[pltpu.VMEM((hidden, 1), F32), pltpu.VMEM((hidden, total_rows), BF)],
        flops=2 * flat,
    )
    own = model // (ep * tp)
    high = -(-(experts + 8) // (8 * (128 // own))) * 8
    routers = jnp.concatenate(
        [router_expert.T, router_group.T, jnp.zeros((8 - groups, model), BF)], axis=0
    )
    merged = call(
        functools.partial(merge_kernel, dims, experts),
        [sds((slots, half))] * groups + [sds((ep // tp, high, 128), F32)] * 2,
        (ids, routers, *back, z_own, *z_tok),
        flops=4 * small,
    )
    b_z, mine, other = merged[:groups], merged[-2], merged[-1]
    b_z = [b_z[0]] + over_groups(b_z[1:])
    other = swap(other)
    part = jnp.where(
        tp_i == 0,
        jnp.concatenate([mine, other], axis=0),
        jnp.concatenate([other, mine], axis=0),
    )
    part = lax.all_to_all(part, "ep", split_axis=0, concat_axis=0, tiled=True)
    by_expert, by_group, router_rows = call(
        functools.partial(reduce_kernel, (experts, groups, own)),
        [sds((experts, own), F32), sds((groups, own), F32), sds((1, own), F32)],
        (part,),
        flops=small // 8,
    )
    token_grad = call(
        functools.partial(final_kernel, (groups, slots)),
        sds((toks, half)),
        (ids, stat, *b_z),
        flops=2 * small,
    )
    gsq = gsq + swap(gsq)
    usq = usq + swap(usq)
    return (
        token_grad,
        gate_grad[None],
        up_grad[None],
        down_grad[None],
        gsq,
        usq,
        dsq,
        by_expert.T,
        by_group.T,
        router_rows.reshape(own),
    )


def solution(mesh):
    return jax.shard_map(
        body,
        mesh=mesh,
        in_specs=(
            P("ep", None),
            P("ep", None),
            P("ep", None),
            P(),
            P(),
            P("ep", None, "tp"),
            P("ep", None, "tp"),
            P("ep", "tp", None),
        ),
        out_specs=(
            P("ep", "tp"),
            P("ep", None, "tp"),
            P("ep", None, "tp"),
            P("ep", "tp", None),
            P("ep", None),
            P("ep", None),
            P("ep", "tp"),
            P(("ep", "tp"), None),
            P(("ep", "tp"), None),
            P(("ep", "tp")),
        ),
        check_vma=False,
    )
```

time: 439 us -> 121 us (0.28)
  waiting for transfers between devices: 293 us -> 46 us
  blocking collectives: 61.5 us -> 0 us
  starting transfers between devices: 7.95 us -> 37.5 us
  Pallas kernels: 0 us -> 27.6 us
  matrix products: 24.5 us -> 0 us
  local copies, waits for them, and re-layouts: 30.1 us -> 5.91 us
  between operations: 14.1 us -> 0.92 us
    unnamed x7 -> x0, waiting for transfers between devices: 270 us -> none
    all_to_all x3 -> x0, blocking collectives: 57.5 us -> none  [the longest x1 34.6 us: body(): lax.all_to_all(part_tok, 'ep', split_axis=0, concat_axis=0, tiled=True)]
    ppermute x0 -> x40, waiting for transfers between devices: none -> 46 us  [the longest x12 31.2 us: over_members(): moved.append(lax.ppermute(blocks[k], 'ep', [(i, i ^ k) for i in range(ep)]))]
    ppermute x0 -> x40, starting transfers between devices: none -> 32.2 us  [the longest x9 14.6 us: over_groups(): moved.append(lax.ppermute(x, 'ep', perm))]
    pallas_call x0 -> x13, Pallas kernels: none -> 27.6 us  [call(): pl.pallas_call(kernel, out_shape=out_shapes, in_specs=in_specs, out_specs...]
    all_to_all x2 -> x1, waiting for transfers between devices: 23.1 us -> 0.01 us  [body(): part = lax.all_to_all(part, 'ep', split_axis=0, concat_axis=0, tiled=True)]
    dot_general x12 -> x0, matrix products: 21.7 us -> none  [the longest x3 9.08 us: contract_rows(): lax.dot_general(left_side, right_side, (((0,), (0,)), ((), ())), preferre...]
    gather x13 -> x0, local copies, waits for them, and re-layouts: 19 us -> none  [the longest x1 6.4 us: body(): jnp.take(tokens, source_rows, axis=0, mode='fill', fill_value=0)]
  transfers between devices with their start and end apart: 7 -> 41, of which waited for: 3 -> 9; matrix products, arithmetic and copies ran while one was open for 8% -> 1% of each run, Pallas kernels for 0% -> 14%
where the time goes in v1:
time: 121 us
  waiting for transfers between devices  46 us (38%)
  starting transfers between devices  37.5 us (31%)
  Pallas kernels  27.6 us (23%)
  local copies, waits for them, and re-layouts  5.91 us (5%)
  other arithmetic  2.6 us (2%)
    ppermute x12, waiting for transfers between devices, over_members(): moved.append(lax.ppermute(blocks[k], 'ep', [(i, i ^ k) for i in range(ep)]))  31.2 us
    pallas_call x13, Pallas kernels, call(): pl.pallas_call(kernel, out_shape=out_shapes, in_specs=in_specs, out_specs...  27.6 us
    ppermute x9, starting transfers between devices, over_groups(): moved.append(lax.ppermute(x, 'ep', perm))  14.6 us
    ppermute x12, starting transfers between devices, over_members(): moved.append(lax.ppermute(blocks[k], 'ep', [(i, i ^ k) for i in range(ep)]))  13.7 us
    ppermute x9, waiting for transfers between devices, over_groups(): moved.append(lax.ppermute(x, 'ep', perm))  13.5 us
    unnamed x32, local copies, waits for them, and re-layouts  5.83 us
    all_to_all x1, starting transfers between devices, body(): part = lax.all_to_all(part, 'ep', split_axis=0, concat_axis=0, tiled=True)  5.3 us
    ppermute x19, starting transfers between devices, swap(): return lax.ppermute(x, 'tp', [(i, tp - 1 - i) for i in range(tp)])  3.88 us
  transfers between devices with their start and end apart: 41, of which 9 were waited for; matrix products, arithmetic and copies ran while one was open for 1% of the time, Pallas kernels for 14%

profile of v1, /device:TPU:0, one launch (start us, length us, event | category | flops | bytes accessed | tf_op | source)
XLA Modules:
  0.0 120.5 jit_solution(6588017998294542449)
XLA Ops:
  1.3 3.8 %shard_map.159 = (bf16[64,1152]{1,0:T(8,128)(2,1)}, bf16[64,1152]{1,0:T(8,128)(2,1)}, bf16[64,1152]{1,0:T(8,128)(2,1)}, bf16[64,1152]{1,0:T(8,128)(2,1)}, bf16[6...) custom-call(s32[4]{0:T(128)} %pad_add_fusion.ids, ...), custom_call_target="tpu_custom_call" | custom-call | flops 134217728 | tf_op jit(solution)/shard_map/pallas_call | solution.py:43
  5.2 3.1 %collective-permute-start.6 = (bf16[64,1024]{1,0:T(8,128)(2,1)}, bf16[64,1024]{1,0:T(8,128)(2,1)S(1)}, u32[]{:S(2)}, u32[]{:S(2)}) collective-permute-start(bf16[64,1024]{1,0:T(8,128)(2,1)} %get-tuple-element.74), channel_id=1, source_target_pairs={{0,8},{2,10},{4,12},{6,14},{8,0},{10,2},{12,4},{14,6},{16,24},{18,... | collective-permute-start | bytes 393224 | tf_op jit(solution)/shard_map/ppermute | solution.py:393
  8.3 2.6 %collective-permute-start.7 = (bf16[64,1024]{1,0:T(8,128)(2,1)}, bf16[64,1024]{1,0:T(8,128)(2,1)S(1)}, u32[]{:S(2)}, u32[]{:S(2)}) collective-permute-start(bf16[64,1024]{1,0:T(8,128)(2,1)} %get-tuple-element.75), channel_id=1, source_target_pairs={{0,16},{2,18},{4,20},{6,22},{8,24},{10,26},{12,28},{14,30},{16,0},... | collective-permute-start | bytes 393224 | tf_op jit(solution)/shard_map/ppermute | solution.py:393
  14.8 2.5 %collective-permute-done.7.refs_4_ = bf16[64,1024]{1,0:T(8,128)(2,1)S(1)} collective-permute-done((bf16[64,1024]{1,0:T(8,128)(2,1)}, bf16[64,1024]{1,0:T(8,128)(2,1)S(1)}, u32[]{:S(2)}, u32[]{:S(2)}) %collective-permute-start.7) | collective-permute-done | bytes 131104 | tf_op jit(solution)/shard_map/ppermute | solution.py:393
  18.0 2.0 %collective-permute-start.5 = (bf16[64,1152]{1,0:T(8,128)(2,1)}, bf16[64,1152]{1,0:T(8,128)(2,1)S(1)}, u32[]{:S(2)}, u32[]{:S(2)}) collective-permute-start(bf16[64,1152]{1,0:T(8,128)(2,1)} %get-tuple-element.73), channel_id=1, source_target_pairs={{0,24},{2,26},{4,28},{6,30},{8,16},{10,18},{12,20},{14,22},{16,8},... | collective-permute-start | bytes 442376 | tf_op jit(solution)/shard_map/ppermute | solution.py:393
  22.1 11.0 %collective-permute-done.4.refs_1_.refs_6_ = bf16[64,1152]{1,0:T(8,128)(2,1)S(1)} collective-permute-done((bf16[64,1152]{1,0:T(8,128)(2,1)}, bf16[64,1152]{1,0:T(8,128)(2,1)S(1)}, u32[]{:S(2)}, u32[]{:S(2)}) %collective-permute-start.4) | collective-permute-done | bytes 147488 | tf_op jit(solution)/shard_map/ppermute | solution.py:393
  40.8 2.5 %collective-permute-start.22 = (bf16[96,1152]{1,0:T(8,128)(2,1)S(1)}, bf16[96,1152]{1,0:T(8,128)(2,1)S(1)}, u32[]{:S(2)}, u32[]{:S(2)}) collective-permute-start(bf16[96,1152]{1,0:T(8,128)(2,1)S(1)} %get-tuple-element.84), channel_id=1, source_target_pairs={{0,6},{2,4},{4,2},{6,0},{8,14},{10,12},{12,10},{14,8},{16,22},{18,... | collective-permute-start | bytes 663560 | tf_op jit(solution)/shard_map/ppermute | solution.py:399
  43.3 4.9 %collective-permute-done.9.refs_5_ = bf16[96,1024]{1,0:T(8,128)(2,1)S(1)} collective-permute-done((bf16[96,1024]{1,0:T(8,128)(2,1)S(1)}, bf16[96,1024]{1,0:T(8,128)(2,1)S(1)}, u32[]{:S(2)}, u32[]{:S(2)}) %collective-permute-start.9) | collective-permute-done | bytes 196640 | tf_op jit(solution)/shard_map/ppermute | solution.py:399
  48.7 6.5 %collective-permute-done.10.refs_6_ = bf16[96,1024]{1,0:T(8,128)(2,1)S(1)} collective-permute-done((bf16[96,1024]{1,0:T(8,128)(2,1)S(1)}, bf16[96,1024]{1,0:T(8,128)(2,1)S(1)}, u32[]{:S(2)}, u32[]{:S(2)}) %collective-permute-start.10) | collective-permute-done | bytes 196640 | tf_op jit(solution)/shard_map/ppermute | solution.py:399
  55.2 6.6 %collective-permute-done.11.refs_7_ = bf16[96,1024]{1,0:T(8,128)(2,1)S(1)} collective-permute-done((bf16[96,1024]{1,0:T(8,128)(2,1)S(1)}, bf16[96,1024]{1,0:T(8,128)(2,1)S(1)}, u32[]{:S(2)}, u32[]{:S(2)}) %collective-permute-start.11) | collective-permute-done | bytes 196640 | tf_op jit(solution)/shard_map/ppermute | solution.py:399
  63.8 1.9 %shard_map.162 = (bf16[512,2048]{1,0:T(8,128)(2,1)S(1)}, f32[512,256]{1,0:T(8,128)S(1)}, f32[512,256]{1,0:T(8,128)S(1)}) custom-call(s32[4]{0:T(128)S(1)} %copy-done.7, bf16[32,2176]{1,0:T(8,128)(2,1)S(1)} %copy-done.5, bf16[32,2176]{1,0:T(8,128)(2,1)S(1)} %collective-permute-done.refs_1_, bf16[32,2176]{1,0:T(8,128)(2,1)S(1)} %collective-permute-done.1.refs_2_, ...), custom_call_target="tpu_custom_call" | custom-call | flops 1073741824 | tf_op jit(solution)/shard_map/pallas_call | solution.py:43
  67.0 1.7 %shard_map.163 = (bf16[512,256]{1,0:T(8,128)(2,1)S(1)}, bf16[512,256]{1,0:T(8,128)(2,1)S(1)}, bf16[512,256]{1,0:T(8,128)(2,1)S(1)}, bf16[512,2048]{1,0:T(8,128)(...) custom-call(s32[4]{0:T(128)S(1)} %copy-done.7, bf16[32,2176]{1,0:T(8,128)(2,1)S(1)} %copy-done.5, ...), custom_call_target="tpu_custom_call" | custom-call | flops 536870912 | tf_op jit(solution)/shard_map/pallas_call | solution.py:43
  68.8 1.9 %shard_map.165 = (bf16[128,1152]{1,0:T(8,128)(2,1)S(1)}, bf16[128,1152]{1,0:T(8,128)(2,1)S(1)}, bf16[128,1152]{1,0:T(8,128)(2,1)S(1)}, bf16[128,1152]{1,0:T(8,128)(2,1)S(1)}) custom-call(s32[4]{0:T(128)S(1)} %copy-done.7, bf16[512,256]{1,0:T(8,128)(2,1)S(1)} %get-tuple-element.87.gd_ref, bf16[512,256]{1,0:T(8,128)(2,1)S(1)} %get-tuple-element.88.ud_ref, ...), custom_call_target="tpu_custom_call" | custom-call | flops 536870912 | tf_op jit(solution)/shard_map/pallas_call | solution.py:43
  71.9 1.9 %shard_map.164 = (bf16[128,1152]{1,0:T(8,128)(2,1)S(1)}, bf16[128,1152]{1,0:T(8,128)(2,1)S(1)}, bf16[128,1152]{1,0:T(8,128)(2,1)S(1)}, bf16[128,1152]{1,0:T(8,128)(2,1)S(1)}) custom-call(s32[4]{0:T(128)S(1)} %copy-done.7, bf16[512,256]{1,0:T(8,128)(2,1)S(1)} %get-tuple-element.87.gd_ref, bf16[512,256]{1,0:T(8,128)(2,1)S(1)} %get-tuple-element.88.ud_ref, ...), custom_call_target="tpu_custom_call" | custom-call | flops 536870912 | tf_op jit(solution)/shard_map/pallas_call | solution.py:43
  76.1 1.9 %collective-permute-start.33 = (bf16[128,1152]{1,0:T(8,128)(2,1)S(1)}, bf16[128,1152]{1,0:T(8,128)(2,1)S(1)}, u32[]{:S(2)}, u32[]{:S(2)}) collective-permute-start(bf16[128,1152]{1,0:T(8,128)(2,1)S(1)} %get-tuple-element.101), channel_id=1, source_target_pairs={{0,6},{2,4},{4,2},{6,0},{8,14},{10,12},{12,10},{14,8},{16,22},{18,... | collective-permute-start | bytes 884744 | tf_op jit(solution)/shard_map/ppermute | solution.py:399
  78.1 6.3 %collective-permute-done.31.refs_1_ = bf16[128,1152]{1,0:T(8,128)(2,1)S(1)} collective-permute-done((bf16[128,1152]{1,0:T(8,128)(2,1)S(1)}, bf16[128,1152]{1,0:T(8,128)(2,1)S(1)}, u32[]{:S(2)}, u32[]{:S(2)}) %collective-permute-start.31) | collective-permute-done | bytes 294944 | tf_op jit(solution)/shard_map/ppermute | solution.py:399
  84.4 6.4 %collective-permute-done.33.refs_3_ = bf16[128,1152]{1,0:T(8,128)(2,1)S(1)} collective-permute-done((bf16[128,1152]{1,0:T(8,128)(2,1)S(1)}, bf16[128,1152]{1,0:T(8,128)(2,1)S(1)}, u32[]{:S(2)}, u32[]{:S(2)}) %collective-permute-start.33) | collective-permute-done | bytes 294944 | tf_op jit(solution)/shard_map/ppermute | solution.py:399
  90.8 1.8 %shard_map.167 = (bf16[64,1024]{1,0:T(8,128)(2,1)S(1)}, bf16[64,1024]{1,0:T(8,128)(2,1)S(1)}, bf16[64,1024]{1,0:T(8,128)(2,1)S(1)}, bf16[64,1024]{1,0:T(8,128)(2...) custom-call(s32[4]{0:T(128)S(1)} %copy-done.7, bf16[24,2048]{1,0:T(8,128)(2,1)S(1)} %maximum_maximum_fusion.rt_ref, ...), custom_call_target="tpu_custom_call" | custom-call | flops 134217728 | tf_op jit(solution)/shard_map/pallas_call | solution.py:43
  95.7 5.3 %all-to-all-start = ((f32[16,16,128]{2,1,0:T(8,128)}), f32[16,16,128]{2,1,0:T(8,128)S(1)}, u32[]{:S(2)}, u32[]{:S(2)}) async-start(f32[16,16,128]{2,1,0:T(8,128)} %maximum_select_fusion), calls=%async_computation | async-start | bytes 262144 | tf_op jit(solution)/shard_map/all_to_all | solution.py:520
  101.1 1.9 %collective-permute-start.34 = (bf16[64,1024]{1,0:T(8,128)(2,1)}, bf16[64,1024]{1,0:T(8,128)(2,1)S(1)}, u32[]{:S(2)}, u32[]{:S(2)}) collective-permute-start(bf16[64,1024]{1,0:T(8,128)(2,1)} %copy-done.13), channel_id=1, source_target_pairs={{0,8},{2,10},{4,12},{6,14},{8,0},{10,2},{12,4},{14,6},{16,24},{18,... | collective-permute-start | bytes 393224 | tf_op jit(solution)/shard_map/ppermute | solution.py:393
  103.0 2.4 %collective-permute-start.35 = (bf16[64,1024]{1,0:T(8,128)(2,1)}, bf16[64,1024]{1,0:T(8,128)(2,1)S(1)}, u32[]{:S(2)}, u32[]{:S(2)}) collective-permute-start(bf16[64,1024]{1,0:T(8,128)(2,1)} %copy-done.12), channel_id=1, source_target_pairs={{0,16},{2,18},{4,20},{6,22},{8,24},{10,26},{12,28},{14,30},{16,0},... | collective-permute-start | bytes 393224 | tf_op jit(solution)/shard_map/ppermute | solution.py:393
  105.5 1.6 %copy-done.11 = bf16[512,2048]{1,0:T(8,128)(2,1)S(1)} copy-done((bf16[512,2048]{1,0:T(8,128)(2,1)S(1)}, bf16[512,2048]{1,0:T(8,128)(2,1)}, u32[]{:S(2)}) %copy-start.11) | copy-done | bytes 2097176
  107.1 5.2 %shard_map.169 = (bf16[2048,256]{1,0:T(8,128)(2,1)}, bf16[2048,256]{1,0:T(8,128)(2,1)}, f32[1,2048]{1,0:T(1,128)S(1)}, f32[1,2048]{1,0:T(1,128)S(1)}) custom-call(bf16[512,2048]{1,0:T(8,128)(2,1)S(1)} %copy-done.11, bf16[512,256]{1,0:T(8,128)(2,1)S(1)} %get-tuple-element.87.gd_ref, bf16[512,256]{1,0:T(8,128)(2,1)S(1)} %get-tuple-element.88.ud_ref), custom_call_target="tpu_custom_call" | custom-call | flops 1073741824 | tf_op jit(solution)/shard_map/pallas_call | solution.py:43
  112.8 4.3 %shard_map.170 = (bf16[256,2048]{1,0:T(8,128)(2,1)}, f32[1,256]{1,0:T(1,128)}) custom-call(bf16[512,2048]{1,0:T(8,128)(2,1)S(1)} %copy-done.3, f32[512,128]{1,0:T(8,128)S(1)} %get-tuple-element.111.w_ref, bf16[512,256]{1,0:T(8,128)(2,1)S(1)} %get-tuple-element.112.hid_ref), custom_call_target="tpu_custom_call" | custom-call | flops 536870912 | tf_op jit(solution)/shard_map/pallas_call | solution.py:43
  (110 shorter events, 29.8 us)
Async XLA Ops:
  5.2 9.2 %collective-permute-start.6 = (bf16[64,1024]{1,0:T(8,128)(2,1)}, bf16[64,1024]{1,0:T(8,128)(2,1)S(1)}, u32[]{:S(2)}, u32[]{:S(2)}) collective-permute-start(bf16[64,1024]{1,0:T(8,128)(2,1)} %get-tuple-element.74), channel_id=1, source_target_pairs={{0,8},{2,10},{4,12},{6,14},{8,0},{10,2},{12,4},{14,6},{16,24},{18,... | collective-permute-start | bytes 393224 | tf_op jit(solution)/shard_map/ppermute | solution.py:393
  8.3 9.0 %collective-permute-start.7 = (bf16[64,1024]{1,0:T(8,128)(2,1)}, bf16[64,1024]{1,0:T(8,128)(2,1)S(1)}, u32[]{:S(2)}, u32[]{:S(2)}) collective-permute-start(bf16[64,1024]{1,0:T(8,128)(2,1)} %get-tuple-element.75), channel_id=1, source_target_pairs={{0,16},{2,18},{4,20},{6,22},{8,24},{10,26},{12,28},{14,30},{16,0},... | collective-permute-start | bytes 393224 | tf_op jit(solution)/shard_map/ppermute | solution.py:393
  12.4 8.3 %collective-permute-start.1 = (bf16[32,2176]{1,0:T(8,128)(2,1)}, bf16[32,2176]{1,0:T(8,128)(2,1)S(1)}, u32[]{:S(2)}, u32[]{:S(2)}) collective-permute-start(bf16[32,2176]{1,0:T(8,128)(2,1)} %get-tuple-element.69), channel_id=1, source_target_pairs={{0,4},{2,6},{4,0},{6,2},{8,12},{10,14},{12,8},{14,10},{16,20},{18,... | collective-permute-start | bytes 417800 | tf_op jit(solution)/shard_map/ppermute | solution.py:399
  17.3 15.7 %collective-permute-start.4 = (bf16[64,1152]{1,0:T(8,128)(2,1)}, bf16[64,1152]{1,0:T(8,128)(2,1)S(1)}, u32[]{:S(2)}, u32[]{:S(2)}) collective-permute-start(bf16[64,1152]{1,0:T(8,128)(2,1)} %get-tuple-element.72), channel_id=1, source_target_pairs={{0,16},{2,18},{4,20},{6,22},{8,24},{10,26},{12,28},{14,30},{16,0},... | collective-permute-start | bytes 442376 | tf_op jit(solution)/shard_map/ppermute | solution.py:393
  18.0 15.0 %collective-permute-start.5 = (bf16[64,1152]{1,0:T(8,128)(2,1)}, bf16[64,1152]{1,0:T(8,128)(2,1)S(1)}, u32[]{:S(2)}, u32[]{:S(2)}) collective-permute-start(bf16[64,1152]{1,0:T(8,128)(2,1)} %get-tuple-element.73), channel_id=1, source_target_pairs={{0,24},{2,26},{4,28},{6,30},{8,16},{10,18},{12,20},{14,22},{16,8},... | collective-permute-start | bytes 442376 | tf_op jit(solution)/shard_map/ppermute | solution.py:393
  20.6 16.5 %collective-permute-start.12 = (bf16[32,2176]{1,0:T(8,128)(2,1)}, bf16[32,2176]{1,0:T(8,128)(2,1)S(1)}, u32[]{:S(2)}, u32[]{:S(2)}) collective-permute-start(bf16[32,2176]{1,0:T(8,128)(2,1)} %get-tuple-element.67.refs_0_), channel_id=1, source_target_pairs={{0,1},{1,0},{2,3},{3,2},{4,5},{5,4},{6,7},{7,6},{8,9},{9,8},{10,11... | collective-permute-start | bytes 417800 | tf_op jit(solution)/shard_map/ppermute | solution.py:403
  20.6 14.9 %collective-permute-start.8 = (bf16[64,1024]{1,0:T(8,128)(2,1)}, bf16[64,1024]{1,0:T(8,128)(2,1)S(1)}, u32[]{:S(2)}, u32[]{:S(2)}) collective-permute-start(bf16[64,1024]{1,0:T(8,128)(2,1)} %get-tuple-element.76), channel_id=1, source_target_pairs={{0,24},{2,26},{4,28},{6,30},{8,16},{10,18},{12,20},{14,22},{16,8},... | collective-permute-start | bytes 393224 | tf_op jit(solution)/shard_map/ppermute | solution.py:393
  21.9 17.8 %collective-permute-start.13 = (bf16[32,2176]{1,0:T(8,128)(2,1)S(1)}, bf16[32,2176]{1,0:T(8,128)(2,1)S(1)}, u32[]{:S(2)}, u32[]{:S(2)}) collective-permute-start(bf16[32,2176]{1,0:T(8,128)(2,1)S(1)} %collective-permute-done.refs_1_), channel_id=1, source_target_pairs={{0,1},{1,0},{2,3},{3,2},{4,5},{5,4},{6,7},{7,6},{8,9},{9,8},{10,11... | collective-permute-start | bytes 417800 | tf_op jit(solution)/shard_map/ppermute | solution.py:403
  33.1 7.8 %collective-permute-start.15 = (bf16[32,2176]{1,0:T(8,128)(2,1)S(1)}, bf16[32,2176]{1,0:T(8,128)(2,1)S(1)}, u32[]{:S(2)}, u32[]{:S(2)}) collective-permute-start(bf16[32,2176]{1,0:T(8,128)(2,1)S(1)} %collective-permute-done.2.refs_3_), channel_id=1, source_target_pairs={{0,1},{1,0},{2,3},{3,2},{4,5},{5,4},{6,7},{7,6},{8,9},{9,8},{10,11... | collective-permute-start | bytes 417800 | tf_op jit(solution)/shard_map/ppermute | solution.py:403
  35.6 12.6 %collective-permute-start.20 = (bf16[96,1152]{1,0:T(8,128)(2,1)S(1)}, bf16[96,1152]{1,0:T(8,128)(2,1)S(1)}, u32[]{:S(2)}, u32[]{:S(2)}) collective-permute-start(bf16[96,1152]{1,0:T(8,128)(2,1)S(1)} %get-tuple-element.82), channel_id=1, source_target_pairs={{0,2},{2,0},{4,6},{6,4},{8,10},{10,8},{12,14},{14,12},{16,18},{18,... | collective-permute-start | bytes 663560 | tf_op jit(solution)/shard_map/ppermute | solution.py:399
  37.1 11.5 %collective-permute-start.21 = (bf16[96,1152]{1,0:T(8,128)(2,1)S(1)}, bf16[96,1152]{1,0:T(8,128)(2,1)S(1)}, u32[]{:S(2)}, u32[]{:S(2)}) collective-permute-start(bf16[96,1152]{1,0:T(8,128)(2,1)S(1)} %get-tuple-element.83), channel_id=1, source_target_pairs={{0,4},{2,6},{4,0},{6,2},{8,12},{10,14},{12,8},{14,10},{16,20},{18,... | collective-permute-start | bytes 663560 | tf_op jit(solution)/shard_map/ppermute | solution.py:399
  39.7 8.4 %collective-permute-start.9 = (bf16[96,1024]{1,0:T(8,128)(2,1)S(1)}, bf16[96,1024]{1,0:T(8,128)(2,1)S(1)}, u32[]{:S(2)}, u32[]{:S(2)}) collective-permute-start(bf16[96,1024]{1,0:T(8,128)(2,1)S(1)} %get-tuple-element.78), channel_id=1, source_target_pairs={{0,2},{2,0},{4,6},{6,4},{8,10},{10,8},{12,14},{14,12},{16,18},{18,... | collective-permute-start | bytes 589832 | tf_op jit(solution)/shard_map/ppermute | solution.py:399
  40.3 14.9 %collective-permute-start.10 = (bf16[96,1024]{1,0:T(8,128)(2,1)S(1)}, bf16[96,1024]{1,0:T(8,128)(2,1)S(1)}, u32[]{:S(2)}, u32[]{:S(2)}) collective-permute-start(bf16[96,1024]{1,0:T(8,128)(2,1)S(1)} %get-tuple-element.79), channel_id=1, source_target_pairs={{0,4},{2,6},{4,0},{6,2},{8,12},{10,14},{12,8},{14,10},{16,20},{18,... | collective-permute-start | bytes 589832 | tf_op jit(solution)/shard_map/ppermute | solution.py:399
  40.8 14.4 %collective-permute-start.22 = (bf16[96,1152]{1,0:T(8,128)(2,1)S(1)}, bf16[96,1152]{1,0:T(8,128)(2,1)S(1)}, u32[]{:S(2)}, u32[]{:S(2)}) collective-permute-start(bf16[96,1152]{1,0:T(8,128)(2,1)S(1)} %get-tuple-element.84), channel_id=1, source_target_pairs={{0,6},{2,4},{4,2},{6,0},{8,14},{10,12},{12,10},{14,8},{16,22},{18,... | collective-permute-start | bytes 663560 | tf_op jit(solution)/shard_map/ppermute | solution.py:399
  48.1 13.7 %collective-permute-start.23 = (bf16[96,1152]{1,0:T(8,128)(2,1)S(1)}, bf16[96,1152]{1,0:T(8,128)(2,1)S(1)}, u32[]{:S(2)}, u32[]{:S(2)}) collective-permute-start(bf16[96,1152]{1,0:T(8,128)(2,1)S(1)} %get-tuple-element.81.refs_4_.refs_16_), channel_id=1, source_target_pairs={{0,1},{1,0},{2,3},{3,2},{4,5},{5,4},{6,7},{7,6},{8,9},{9,8},{10,11... | collective-permute-start | bytes 663560 | tf_op jit(solution)/shard_map/ppermute | solution.py:403
  48.1 14.2 %collective-permute-start.24 = (bf16[96,1152]{1,0:T(8,128)(2,1)S(1)}, bf16[96,1152]{1,0:T(8,128)(2,1)S(1)}, u32[]{:S(2)}, u32[]{:S(2)}) collective-permute-start(bf16[96,1152]{1,0:T(8,128)(2,1)S(1)} %collective-permute-done.20.refs_5_.refs_17_), channel_id=1, source_target_pairs={{0,1},{1,0},{2,3},{3,2},{4,5},{5,4},{6,7},{7,6},{8,9},{9,8},{10,11... | collective-permute-start | bytes 663560 | tf_op jit(solution)/shard_map/ppermute | solution.py:403
  48.7 13.7 %collective-permute-start.25 = (bf16[96,1152]{1,0:T(8,128)(2,1)S(1)}, bf16[96,1152]{1,0:T(8,128)(2,1)S(1)}, u32[]{:S(2)}, u32[]{:S(2)}) collective-permute-start(bf16[96,1152]{1,0:T(8,128)(2,1)S(1)} %collective-permute-done.21.refs_6_.refs_18_), channel_id=1, source_target_pairs={{0,1},{1,0},{2,3},{3,2},{4,5},{5,4},{6,7},{7,6},{8,9},{9,8},{10,11... | collective-permute-start | bytes 663560 | tf_op jit(solution)/shard_map/ppermute | solution.py:403
  74.4 9.9 %collective-permute-start.31 = (bf16[128,1152]{1,0:T(8,128)(2,1)S(1)}, bf16[128,1152]{1,0:T(8,128)(2,1)S(1)}, u32[]{:S(2)}, u32[]{:S(2)}) collective-permute-start(bf16[128,1152]{1,0:T(8,128)(2,1)S(1)} %get-tuple-element.99), channel_id=1, source_target_pairs={{0,2},{2,0},{4,6},{6,4},{8,10},{10,8},{12,14},{14,12},{16,18},{18,... | collective-permute-start | bytes 884744 | tf_op jit(solution)/shard_map/ppermute | solution.py:399
  74.5 9.8 %collective-permute-start.32 = (bf16[128,1152]{1,0:T(8,128)(2,1)S(1)}, bf16[128,1152]{1,0:T(8,128)(2,1)S(1)}, u32[]{:S(2)}, u32[]{:S(2)}) collective-permute-start(bf16[128,1152]{1,0:T(8,128)(2,1)S(1)} %get-tuple-element.100), channel_id=1, source_target_pairs={{0,4},{2,6},{4,0},{6,2},{8,12},{10,14},{12,8},{14,10},{16,20},{18,... | collective-permute-start | bytes 884744 | tf_op jit(solution)/shard_map/ppermute | solution.py:399
  76.1 14.7 %collective-permute-start.33 = (bf16[128,1152]{1,0:T(8,128)(2,1)S(1)}, bf16[128,1152]{1,0:T(8,128)(2,1)S(1)}, u32[]{:S(2)}, u32[]{:S(2)}) collective-permute-start(bf16[128,1152]{1,0:T(8,128)(2,1)S(1)} %get-tuple-element.101), channel_id=1, source_target_pairs={{0,6},{2,4},{4,2},{6,0},{8,14},{10,12},{12,10},{14,8},{16,22},{18,... | collective-permute-start | bytes 884744 | tf_op jit(solution)/shard_map/ppermute | solution.py:399
  95.7 24.1 %all-to-all-start = ((f32[16,16,128]{2,1,0:T(8,128)}), f32[16,16,128]{2,1,0:T(8,128)S(1)}, u32[]{:S(2)}, u32[]{:S(2)}) async-start(f32[16,16,128]{2,1,0:T(8,128)} %maximum_select_fusion), calls=%async_computation | async-start | bytes 262144 | tf_op jit(solution)/shard_map/all_to_all | solution.py:520
  101.1 17.3 %collective-permute-start.34 = (bf16[64,1024]{1,0:T(8,128)(2,1)}, bf16[64,1024]{1,0:T(8,128)(2,1)S(1)}, u32[]{:S(2)}, u32[]{:S(2)}) collective-permute-start(bf16[64,1024]{1,0:T(8,128)(2,1)} %copy-done.13), channel_id=1, source_target_pairs={{0,8},{2,10},{4,12},{6,14},{8,0},{10,2},{12,4},{14,6},{16,24},{18,... | collective-permute-start | bytes 393224 | tf_op jit(solution)/shard_map/ppermute | solution.py:393
  103.0 15.4 %collective-permute-start.35 = (bf16[64,1024]{1,0:T(8,128)(2,1)}, bf16[64,1024]{1,0:T(8,128)(2,1)S(1)}, u32[]{:S(2)}, u32[]{:S(2)}) collective-permute-start(bf16[64,1024]{1,0:T(8,128)(2,1)} %copy-done.12), channel_id=1, source_target_pairs={{0,16},{2,18},{4,20},{6,22},{8,24},{10,26},{12,28},{14,30},{16,0},... | collective-permute-start | bytes 393224 | tf_op jit(solution)/shard_map/ppermute | solution.py:393
  105.3 13.0 %collective-permute-start.36 = (bf16[64,1024]{1,0:T(8,128)(2,1)S(1)}, bf16[64,1024]{1,0:T(8,128)(2,1)S(1)}, u32[]{:S(2)}, u32[]{:S(2)}) collective-permute-start(bf16[64,1024]{1,0:T(8,128)(2,1)S(1)} %get-tuple-element.106), channel_id=1, source_target_pairs={{0,24},{2,26},{4,28},{6,30},{8,16},{10,18},{12,20},{14,22},{16,8},... | collective-permute-start | bytes 393224 | tf_op jit(solution)/shard_map/ppermute | solution.py:393
  (33 other events, 284.1 us)

commit v2 on v1

v2 whole, which is shorter than its diff:
```python
import functools

import jax
import jax.numpy as jnp
from jax import lax
from jax.experimental import pallas as pl
from jax.experimental.pallas import tpu as pltpu
from jax.sharding import PartitionSpec as P


BF = jnp.bfloat16
F32 = jnp.float32


def dot(a, b):
    return jnp.dot(a, b, preferred_element_type=F32)


def dot_nt(a, b):
    return lax.dot_general(a, b, (((1,), (1,)), ((), ())), preferred_element_type=F32)


def dot_tn(a, b):
    return lax.dot_general(a, b, (((0,), (0,)), ((), ())), preferred_element_type=F32)


def iota(shape, axis):
    return lax.broadcasted_iota(jnp.int32, shape, axis)


def onehot(mask):
    return jnp.where(mask, 1.0, 0.0).astype(BF)


def where_am_i(width):
    ep, tp = lax.axis_index("ep"), lax.axis_index("tp")
    return ep // width, ep % width, tp


def call(kernel, out_shapes, args, scratch=(), flops=0, in_hbm=(), limit=24 * 2**20):
    vmem = pl.BlockSpec(memory_space=pltpu.VMEM)
    smem = pl.BlockSpec(memory_space=pltpu.SMEM)
    hbm = pl.BlockSpec(memory_space=pltpu.HBM)
    in_specs = [
        smem if a.ndim == 1 and a.dtype == jnp.int32 else hbm if i in in_hbm else vmem
        for i, a in enumerate(args)
    ]
    return pl.pallas_call(
        kernel,
        out_shape=out_shapes,
        in_specs=in_specs,
        out_specs=jax.tree.map(lambda _: vmem, out_shapes),
        scratch_shapes=list(scratch),
        cost_estimate=pl.CostEstimate(flops=flops, bytes_accessed=0, transcendentals=0),
        compiler_params=pltpu.CompilerParams(vmem_limit_bytes=limit),
    )(*args)


def group_onehots(rank_row, group_row, my_group, ks, slots):
    toks = rank_row.shape[1]
    hit = iota((slots, toks), 0).astype(F32) == rank_row
    outs = []
    for k in ks:
        other = jnp.bitwise_xor(my_group, k).astype(F32)
        outs.append(onehot(jnp.logical_and(hit, group_row == other)))
    return jnp.concatenate(outs, axis=0)


def slot_hits(shape, member, cap, per, s0, s1, slot_axis):
    slot = iota(shape, slot_axis)
    block = slot // per
    want = (jnp.bitwise_xor(member, block) * cap + slot % cap + 1).astype(F32)
    return s0 == want, s1 == want


def prep_kernel(dims, tok_hbm, cot_hbm, routes_hbm, rg_hbm, re_hbm, *rest):
    groups, width, cap, slots = dims
    near_ref, tok_out, cot_out, stat_ref, tok_ref, cot_ref, routes_ref, rg_ref, re_ref, sems = rest
    toks, model = tok_ref.shape
    experts = re_ref.shape[0]
    my_group, _, core = where_am_i(width)
    copies = [
        pltpu.make_async_copy(src, dst, sems.at[i])
        for i, (src, dst) in enumerate(
            (
                (routes_hbm, routes_ref),
                (re_hbm, re_ref),
                (rg_hbm, rg_ref),
                (tok_hbm, tok_ref),
                (cot_hbm, cot_ref),
            )
        )
    ]
    for copy in copies:
        copy.start()
    earlier = onehot(iota((toks, toks), 0) < iota((toks, toks), 1))
    for copy in copies[:4]:
        copy.wait()
    tokens = tok_ref[...]
    e_t = dot_nt(re_ref[...], tokens)
    g_t = dot_nt(rg_ref[...], tokens)
    g_t = jnp.concatenate([g_t, jnp.zeros((8 - groups, toks), F32)], axis=0)
    routes = routes_ref[...].astype(F32)
    r0, r1 = routes[0:1], routes[1:2]
    grow = iota((8, toks), 0)
    gexp = jnp.where(grow < groups, jnp.exp(g_t), 0.0)
    gprob = gexp / jnp.sum(gexp, axis=0, keepdims=True)
    low = (grow * width).astype(F32)
    gmask = jnp.logical_and(r0 >= low, r0 < low + width)
    picked = jnp.sum(jnp.where(gmask, gprob, 0.0), axis=0, keepdims=True)
    group_row = jnp.sum(jnp.where(gmask, grow.astype(F32), 0.0), axis=0, keepdims=True)
    erow = iota((experts, toks), 0).astype(F32)
    a0, a1 = erow == r0, erow == r1
    eexp = jnp.exp(e_t)
    x0 = jnp.sum(jnp.where(a0, eexp, 0.0), axis=0, keepdims=True)
    x1 = jnp.sum(jnp.where(a1, eexp, 0.0), axis=0, keepdims=True)
    p0, p1 = x0 / (x0 + x1), x1 / (x0 + x1)
    cum = dot(onehot(jnp.logical_or(a0, a1)), earlier)
    rank0 = jnp.sum(jnp.where(a0, cum, 0.0), axis=0, keepdims=True)
    rank1 = jnp.sum(jnp.where(a1, cum, 0.0), axis=0, keepdims=True)
    gcum = dot(onehot(gmask), earlier)
    rank_g = jnp.sum(jnp.where(gmask, gcum, 0.0), axis=0, keepdims=True)
    base = group_row * width
    s0 = (r0 - base) * cap + rank0 + 1.0
    s1 = (r1 - base) * cap + rank1 + 1.0
    mrow = iota((128, toks), 0)
    meta = jnp.where(mrow == 0, picked * p0, 0.0)
    meta = jnp.where(mrow == 1, picked * p1, meta)
    meta = jnp.where(mrow == 2, s0, meta)
    meta = jnp.where(mrow == 3, s1, meta)
    for i, v in enumerate([picked, p0, p1] + [gprob[j : j + 1] for j in range(groups)]):
        top = v.astype(BF).astype(F32)
        meta = jnp.where(mrow == 4 + 2 * i, top, meta)
        meta = jnp.where(mrow == 5 + 2 * i, v - top, meta)
    meta = meta.astype(BF)
    stat_ref[...] = jnp.where(iota((8, toks), 0) == 0, rank_g, group_row)
    every = group_onehots(rank_g, group_row, my_group, (core, groups - 1 - core), slots)
    metas = dot_nt(every, meta).astype(BF)
    moved = dot(every, tokens).astype(BF)
    near_ref[:, :model] = moved[:slots]
    tok_out[:, :model] = moved[slots:]
    near_ref[:, 2 * model :] = metas[:slots]
    tok_out[:, model:] = metas[slots:]
    copies[4].wait()
    moved = dot(every, cot_ref[...]).astype(BF)
    near_ref[:, model : 2 * model] = moved[:slots]
    cot_out[...] = moved[slots:]


def spread_kernel(dims, meta_ref, *refs):
    _, width, cap, slots = dims
    member = where_am_i(width)[1]
    data, outs = refs[: len(refs) - width], refs[len(refs) - width :]
    tail = meta_ref.shape[1] - 128
    meta = meta_ref[:, tail:]
    rows = jnp.transpose(jnp.concatenate([meta.astype(F32), jnp.zeros((128 - slots, 128), F32)], axis=0))
    rows = rows[:, :slots]
    shape = (width * cap, slots)
    hit0, hit1 = slot_hits(shape, member, cap, cap, rows[2:3], rows[3:4], 0)
    hit0, hit1 = onehot(hit0), onehot(hit1)
    values = data[0][...] if data else meta_ref[:, :tail]
    spread = dot(hit0 + hit1, values).astype(BF)
    for k in range(width):
        outs[k][:, : values.shape[1]] = spread[k * cap : (k + 1) * cap]
    if not data:
        weight = dot(hit0, meta)[:, 0:1] + dot(hit1, meta)[:, 1:2]
        wide = jnp.broadcast_to(weight, (width * cap, 128)).astype(BF)
        for k in range(width):
            outs[k][:, tail:] = wide[k * cap : (k + 1) * cap]


def forward_kernel(width, *refs):
    first, second = refs[:width], refs[width : 2 * width]
    weights, x_ref, outs = refs[2 * width : 2 * width + 4], refs[-5], refs[-4:]
    model = x_ref.shape[1]
    cap = first[0].shape[0]
    for k in range(width):
        x_ref[k * cap : (k + 1) * cap, :] = first[k][:, :model]
        x_ref[(width + k) * cap : (width + k + 1) * cap, :] = second[k][:, :model]
    x = x_ref[...]
    for w, out in zip(weights, outs):
        out[...] = dot(x, w[...])


def delta_kernel(width, *refs):
    first, second, tok = refs[:width], refs[width : 2 * width], refs[2 * width : 3 * width]
    gates, ups, downs = refs[3 * width : 3 * width + 2], refs[3 * width + 2 : 3 * width + 4], refs[3 * width + 4 : 3 * width + 6]
    gps, upps = refs[3 * width + 6 : 3 * width + 8], refs[3 * width + 8 : 3 * width + 10]
    outs = refs[3 * width + 10 :]
    mine_ref, other_ref, c_ref, w_ref = outs[:4]
    backs = outs[4 : 4 + width]
    model = c_ref.shape[1]
    cap = first[0].shape[0]
    for k in range(width):
        low, up = slice(k * cap, (k + 1) * cap), slice((width + k) * cap, (width + k + 1) * cap)
        c_ref[low, :] = first[k][:, model : 2 * model]
        c_ref[up, :] = second[k][...]
        w_ref[low, :] = first[k][:, 2 * model :].astype(F32)
        w_ref[up, :] = tok[k][:, model:].astype(F32)
    c = c_ref[...]
    scale = w_ref[:, 0:1]
    hidden = gates[0].shape[1]
    s = None
    for n, out in enumerate((mine_ref, other_ref)):
        pulled = dot_nt(c, downs[n][...])
        gate_pre, up_pre = gps[n][...], upps[n][...]
        sig = 1.0 / (1.0 + jnp.exp(-gate_pre))
        silu = gate_pre * sig
        hid = (silu * up_pre).astype(BF)
        dh = scale * pulled
        out[:, :hidden] = (dh * up_pre * sig * (1.0 + gate_pre * (1.0 - sig))).astype(BF)
        out[:, hidden : 2 * hidden] = (dh * silu).astype(BF)
        out[:, 2 * hidden :] = hid
        part = jnp.sum(pulled * hid.astype(F32), axis=1, keepdims=True)
        s = part if s is None else s + part
    wide = jnp.broadcast_to(s, (s.shape[0], 128)).astype(BF)
    for k in range(width):
        backs[k][:cap, model:] = wide[k * cap : (k + 1) * cap]
        backs[k][cap:, model:] = wide[(width + k) * cap : (width + k + 1) * cap]
    step = 256

    @pl.loop(0, model // step)
    def _(i):
        at = pl.ds(pl.multiple_of(i * step, step), step)
        term = None
        for n, out in enumerate((mine_ref, other_ref)):
            piece = dot_nt(out[:, :hidden], gates[n][at, :])
            piece += dot_nt(out[:, hidden : 2 * hidden], ups[n][at, :])
            term = piece if term is None else term + piece
        term = term.astype(BF)
        for k in range(width):
            backs[k][:cap, at] = term[k * cap : (k + 1) * cap]
            backs[k][cap:, at] = term[(width + k) * cap : (width + k + 1) * cap]


def scale_kernel(c_ref, w_ref, out_ref):
    out_ref[...] = (w_ref[:, 0:1] * c_ref[...].astype(F32)).astype(BF)


def fold(x):
    total = x[:, :128]
    for i in range(1, x.shape[1] // 128):
        total = total + x[:, i * 128 : (i + 1) * 128]
    return total


def grad_kernel(x_ref, other_ref, mine_ref, got_ref, gg_ref, ug_ref, sq_ref, gd_ref, ud_ref):
    rows, hidden = x_ref.shape[0], gd_ref.shape[1]
    for n, ref in enumerate((mine_ref, got_ref)):
        gd_ref[n * rows : (n + 1) * rows, :] = ref[:, :hidden]
        ud_ref[n * rows : (n + 1) * rows, :] = ref[:, hidden : 2 * hidden]
    step = 512

    @pl.loop(0, x_ref.shape[1] // step)
    def _(i):
        at = pl.ds(pl.multiple_of(i * step, step), step)
        xt = jnp.concatenate(
            [jnp.transpose(x_ref[:, at]), jnp.transpose(other_ref[:, at])], axis=1
        )
        for n, (d_ref, out) in enumerate(((gd_ref, gg_ref), (ud_ref, ug_ref))):
            total = dot(xt, d_ref[...])
            out[at, :] = total.astype(BF)
            part = jnp.transpose(fold(total * total))
            sq_ref[n : n + 1, at] = jnp.sum(part, axis=0, keepdims=True)


def down_kernel(c_ref, other_ref, mine_ref, got_ref, out_ref, sq_ref, acc, hid_t):
    rows, hidden = c_ref.shape[0], hid_t.shape[0]
    acc[...] = jnp.zeros_like(acc)
    hid_t[:, :rows] = jnp.transpose(mine_ref[:, 2 * hidden :])
    hid_t[:, rows:] = jnp.transpose(got_ref[:, 2 * hidden :])
    step = 512

    @pl.loop(0, c_ref.shape[1] // step)
    def _(i):
        at = pl.ds(pl.multiple_of(i * step, step), step)
        total = dot(hid_t[...], jnp.concatenate([c_ref[:, at], other_ref[:, at]], axis=0))
        out_ref[:, at] = total.astype(BF)
        acc[...] += fold(total * total)

    sq_ref[...] = jnp.sum(jnp.transpose(acc[...]), axis=0, keepdims=True)


def reduce_kernel(dims, got_ref, sq_ref, sq_other_ref, e_ref, g_ref, rows_ref, gsq_ref, usq_ref):
    experts, groups, own = dims
    total = jnp.sum(got_ref[...], axis=0)
    pack = 128 // own
    total = jnp.concatenate([total[:, i * own : (i + 1) * own] for i in range(pack)], axis=0)
    by_expert, by_group = total[:experts], total[experts : experts + groups]
    e_ref[...] = by_expert
    g_ref[...] = by_group
    rows_ref[...] = jnp.sum(by_expert * by_expert, axis=0, keepdims=True) + jnp.sum(
        by_group * by_group, axis=0, keepdims=True
    )
    gsq_ref[...] = sq_ref[0:1] + sq_other_ref[0:1]
    usq_ref[...] = sq_ref[1:2] + sq_other_ref[1:2]


def merge_kernel(dims, experts, rt_ref, near_ref, tok_ref, *refs):
    groups, width, cap, slots = dims
    blocks, (y0_ref, y1_ref, mine_ref, other_ref) = refs[:width], refs[width:]
    my_group, member, core = where_am_i(width)
    model = y0_ref.shape[1]
    meta = jnp.concatenate([near_ref[:, 2 * model :], tok_ref[:, model:]], axis=0).astype(F32)
    toks = 2 * slots
    shape = (toks, width * 2 * cap)
    same = iota(shape, 1) // cap % 2 == iota(shape, 0) // slots
    hit0, hit1 = slot_hits(shape, member, cap, 2 * cap, meta[:, 2:3], meta[:, 3:4], 1)
    hit0, hit1 = onehot(jnp.logical_and(same, hit0)), onehot(jnp.logical_and(same, hit1))
    sent = jnp.concatenate([r[:, model:] for r in blocks], axis=0)
    lane = iota(meta.shape, 1)
    meta = jnp.where(lane == 126, dot(hit0, sent), meta)
    meta = jnp.where(lane == 127, dot(hit1, sent), meta)
    rows = jnp.transpose(meta)
    picked, p0, p1 = [rows[4 + 2 * i : 5 + 2 * i] + rows[5 + 2 * i : 6 + 2 * i] for i in range(3)]
    s0, s1 = rows[126:127], rows[127:128]
    dpicked = s0 * p0 + s1 * p1
    q0, q1 = picked * s0, picked * s1
    mean = p0 * q0 + p1 * q1
    c0, c1 = p0 * (q0 - mean), p1 * (q1 - mean)
    grow = iota((8, toks), 0)
    dgroup = jnp.zeros((8, toks), F32)
    for j in range(groups):
        at = 10 + 2 * j
        prob = rows[at : at + 1] + rows[at + 1 : at + 2]
        hot = jnp.where(my_group == j, 1.0, 0.0)
        dgroup = jnp.where(grow == j, dpicked * picked * (hot - prob), dgroup)
    erow = ((iota((experts, toks), 0) - my_group * width) * cap).astype(F32)
    dexpert = jnp.zeros((experts, toks), F32)
    for c, slot in ((c0, rows[2:3]), (c1, rows[3:4])):
        inside = jnp.logical_and(slot > erow, slot <= erow + cap)
        dexpert += jnp.where(inside, c, 0.0)
    d = jnp.concatenate([dexpert, dgroup], axis=0).astype(BF)
    total = dot(hit0 + hit1, jnp.concatenate([r[:, :model] for r in blocks], axis=0))
    total += dot_tn(d, rt_ref[...])
    y0_ref[...] = total[:slots].astype(BF)
    y1_ref[...] = total[slots:].astype(BF)
    part = dot(d, jnp.concatenate([near_ref[:, :model], tok_ref[:, :model]], axis=0))
    count, high = mine_ref.shape[:2]
    own = model // (2 * count)
    pack = 128 // own
    part = jnp.concatenate([part, jnp.zeros((high * pack - part.shape[0], model), F32)], axis=0)
    for j in range(count):
        low = part[:, 2 * j * own : (2 * j + 1) * own]
        up = part[:, (2 * j + 1) * own : (2 * j + 2) * own]
        for ref, cols in (
            (mine_ref, jnp.where(core == 0, low, up)),
            (other_ref, jnp.where(core == 0, up, low)),
        ):
            ref[j] = jnp.concatenate(
                [cols[i * high : (i + 1) * high] for i in range(pack)], axis=1
            )


def collect_kernel(dims, stat_ref, y0_ref, y1_ref, mine_ref, other_ref):
    groups, width, _, slots = dims
    my_group, _, core = where_am_i(width)
    every = group_onehots(
        stat_ref[0:1, :], stat_ref[1:2, :], my_group, (core, groups - 1 - core), slots
    )
    total = dot_tn(every, jnp.concatenate([y0_ref[...], y1_ref[...]], axis=0)).astype(BF)
    half = mine_ref.shape[1]
    left, right = total[:, :half], total[:, half:]
    mine_ref[...] = jnp.where(core == 0, left, right)
    other_ref[...] = jnp.where(core == 0, right, left)


def final_kernel(mine_ref, other_ref, out_ref):
    out_ref[...] = (mine_ref[...].astype(F32) + other_ref[...].astype(F32)).astype(BF)


def body(tokens, cotangent, routes, router_group, router_expert, gate_proj, up_proj, down_proj):
    toks, model = tokens.shape
    top = routes.shape[1]
    groups = router_group.shape[1]
    experts = router_expert.shape[1]
    width = experts // groups
    cap = toks // width
    slots = width * cap // top
    ep = lax.axis_size("ep")
    tp = lax.axis_size("tp")
    half = model // tp
    hidden = gate_proj.shape[2]
    assert groups == 2 * tp and tp == 2
    dims = (groups, width, cap, slots)
    batch = 2 * width * cap
    flat = batch * model * hidden
    small = toks * toks * model

    def sds(shape, dtype=BF):
        return jax.ShapeDtypeStruct(shape, dtype)

    def over_groups(x, far):
        perm = []
        for i in range(ep):
            for c in range(tp):
                k = groups - 1 - c if far else c
                to = ((i // width) ^ k) * width + i % width
                perm.append((i * tp + c, to * tp + c))
        return lax.ppermute(x, ("ep", "tp"), perm)

    def over_members(blocks):
        moved = [blocks[0]]
        for k in range(1, width):
            moved.append(lax.ppermute(blocks[k], "ep", [(i, i ^ k) for i in range(ep)]))
        return moved

    def swap(x):
        return lax.ppermute(x, "tp", [(i, tp - 1 - i) for i in range(tp)])

    near, z_t, z_c, stat = call(
        functools.partial(prep_kernel, dims),
        [
            sds((slots, 2 * model + 128)),
            sds((slots, model + 128)),
            sds((slots, model)),
            sds((8, toks), F32),
        ],
        (tokens, cotangent, routes.T, router_group.T, router_expert.T),
        scratch=[
            pltpu.VMEM((toks, model), BF),
            pltpu.VMEM((toks, model), BF),
            pltpu.VMEM((top, toks), jnp.int32),
            pltpu.VMEM((groups, model), BF),
            pltpu.VMEM((experts, model), BF),
            pltpu.SemaphoreType.DMA((5,)),
        ],
        in_hbm=(0, 1, 2, 3, 4),
        limit=60 * 2**20,
        flops=4 * small,
    )
    z_t = over_groups(z_t, True)
    near = over_groups(near, False)
    z_c = over_groups(z_c, True)

    def spread(blocks, cols):
        return call(
            functools.partial(spread_kernel, dims),
            [sds((cap, cols))] * width,
            blocks,
            flops=4 * small,
        )

    m_a = over_members(spread((near,), 2 * model + 128))
    m_t = over_members(spread((z_t,), model + 128))
    m_c = over_members(spread((z_t, z_c), model))
    gate_mat, up_mat, down_mat = gate_proj[0], up_proj[0], down_proj[0]
    gates = (gate_mat, swap(gate_mat))
    ups = (up_mat, swap(up_mat))
    downs = (down_mat, swap(down_mat))
    x_full, *pre = call(
        functools.partial(forward_kernel, width),
        [sds((batch, model))] + [sds((batch, hidden), F32)] * 4,
        (*m_a, *m_t, *gates, *ups),
        flops=8 * flat,
    )
    mine, other, c_full, w_cols, *back = call(
        functools.partial(delta_kernel, width),
        [sds((batch, 3 * hidden))] * 2
        + [sds((batch, model)), sds((batch, 128), F32)]
        + [sds((2 * cap, model + 128))] * width,
        (*m_a, *m_c, *m_t, *gates, *ups, *downs, *pre),
        flops=12 * flat,
    )
    back = over_members(back)
    got = swap(other)
    x_other = swap(x_full)
    scaled = call(scale_kernel, sds((batch, model)), (c_full, w_cols), flops=small)
    scaled_other = swap(scaled)
    gate_grad, up_grad, in_sq = call(
        grad_kernel,
        [sds((model, hidden))] * 2 + [sds((2, model), F32)],
        (x_full, x_other, mine, got),
        scratch=[pltpu.VMEM((2 * batch, hidden), BF)] * 2,
        flops=8 * flat,
    )
    down_grad, dsq = call(
        down_kernel,
        [sds((hidden, model)), sds((1, hidden), F32)],
        (scaled, scaled_other, mine, got),
        scratch=[pltpu.VMEM((hidden, 128), F32), pltpu.VMEM((hidden, 2 * batch), BF)],
        flops=4 * flat,
    )
    own = model // (ep * tp)
    high = -(-(experts + 8) // (8 * (128 // own))) * 8
    routers = jnp.concatenate(
        [router_expert.T, router_group.T, jnp.zeros((8 - groups, model), BF)], axis=0
    )
    y_near, y_far, part, part_other = call(
        functools.partial(merge_kernel, dims, experts),
        [sds((slots, model))] * 2 + [sds((ep, high, 128), F32)] * 2,
        (routers, near, z_t, *back),
        flops=4 * small,
    )
    y_far = over_groups(y_far, True)
    y_near = over_groups(y_near, False)
    part = part + swap(part_other)
    part = lax.all_to_all(part, "ep", split_axis=0, concat_axis=0, tiled=True)
    by_expert, by_group, router_rows, gsq, usq = call(
        functools.partial(reduce_kernel, (experts, groups, own)),
        [sds((experts, own), F32), sds((groups, own), F32), sds((1, own), F32)]
        + [sds((1, model), F32)] * 2,
        (part, in_sq, swap(in_sq)),
        flops=small // 8,
    )
    left, right = call(
        functools.partial(collect_kernel, dims),
        [sds((toks, half))] * 2,
        (stat, y_near, y_far),
        flops=2 * small,
    )
    token_grad = call(final_kernel, sds((toks, half)), (left, swap(right)), flops=small)
    return (
        token_grad,
        gate_grad[None],
        up_grad[None],
        down_grad[None],
        gsq,
        usq,
        dsq,
        by_expert.T,
        by_group.T,
        router_rows.reshape(own),
    )


def solution(mesh):
    return jax.shard_map(
        body,
        mesh=mesh,
        in_specs=(
            P("ep", None),
            P("ep", None),
            P("ep", None),
            P(),
            P(),
            P("ep", None, "tp"),
            P("ep", None, "tp"),
            P("ep", "tp", None),
        ),
        out_specs=(
            P("ep", "tp"),
            P("ep", None, "tp"),
            P("ep", None, "tp"),
            P("ep", "tp", None),
            P("ep", None),
            P("ep", None),
            P("ep", "tp"),
            P(("ep", "tp"), None),
            P(("ep", "tp"), None),
            P(("ep", "tp")),
        ),
        check_vma=False,
    )
```

time: 121 us -> 122 us (level)
  starting transfers between devices: 37.5 us -> 49.4 us
  Pallas kernels: 27.6 us -> 22 us
  local copies, waits for them, and re-layouts: 5.91 us -> 0.62 us
  other arithmetic: 2.6 us -> 0.75 us
  waiting for transfers between devices: 46 us -> 47.7 us
    ppermute x19 -> x9, starting transfers between devices: 3.88 us -> 11.7 us  [swap(): return lax.ppermute(x, 'tp', [(i, tp - 1 - i) for i in range(tp)])]
    pallas_call x13, Pallas kernels: 27.6 us -> 22 us  [call(): pl.pallas_call(kernel, out_shape=out_shapes, in_specs=in_specs, out_specs...]
    unnamed x32 -> x12, local copies, waits for them, and re-layouts: 5.83 us -> 0.54 us
    ppermute x12, starting transfers between devices: 13.7 us -> 18.3 us  [over_members(): moved.append(lax.ppermute(blocks[k], 'ep', [(i, i ^ k) for i in range(ep)]))]
    ppermute x12, waiting for transfers between devices: 31.2 us -> 33.9 us  [over_members(): moved.append(lax.ppermute(blocks[k], 'ep', [(i, i ^ k) for i in range(ep)]))]
    ppermute x9 -> x5, waiting for transfers between devices: 13.5 us -> 12.2 us  [over_groups(): return lax.ppermute(x, ('ep', 'tp'), perm)]
    ppermute x9 -> x5, starting transfers between devices: 14.6 us -> 14.9 us  [over_groups(): return lax.ppermute(x, ('ep', 'tp'), perm)]
  transfers between devices with their start and end apart: 41 -> 27, of which waited for: 9 -> 11; matrix products, arithmetic and copies ran while one was open for 1% -> 1% of each run, Pallas kernels for 14% -> 15%
where the time goes in v2:
time: 122 us; the launch traced here: 121 us
  starting transfers between devices  49.4 us (40%)
  waiting for transfers between devices  47.7 us (39%)
  Pallas kernels  22 us (18%)
    ppermute x12, waiting for transfers between devices, over_members(): moved.append(lax.ppermute(blocks[k], 'ep', [(i, i ^ k) for i in range(ep)]))  33.9 us
    pallas_call x13, Pallas kernels, call(): pl.pallas_call(kernel, out_shape=out_shapes, in_specs=in_specs, out_specs...  22 us
    ppermute x12, starting transfers between devices, over_members(): moved.append(lax.ppermute(blocks[k], 'ep', [(i, i ^ k) for i in range(ep)]))  18.3 us
    ppermute x5, starting transfers between devices, over_groups(): return lax.ppermute(x, ('ep', 'tp'), perm)  14.9 us
    ppermute x5, waiting for transfers between devices, over_groups(): return lax.ppermute(x, ('ep', 'tp'), perm)  12.2 us
    ppermute x9, starting transfers between devices, swap(): return lax.ppermute(x, 'tp', [(i, tp - 1 - i) for i in range(tp)])  11.7 us
    all_to_all x1, starting transfers between devices, body(): part = lax.all_to_all(part, 'ep', split_axis=0, concat_axis=0, tiled=True)  4.46 us
  transfers between devices with their start and end apart: 27, of which 11 were waited for; matrix products, arithmetic and copies ran while one was open for 1% of the time, Pallas kernels for 15%

profile of v2, /device:TPU:0, one launch (start us, length us, event | category | flops | bytes accessed | tf_op | source)
XLA Modules:
  0.0 121.2 jit_solution(11149129693583794579)
XLA Ops:
  0.7 3.1 %shard_map.159 = (bf16[64,4224]{1,0:T(8,128)(2,1)}, bf16[64,2176]{1,0:T(8,128)(2,1)}, bf16[64,2048]{1,0:T(8,128)(2,1)}, f32[8,128]{1,0:T(8,128)}) custom-call(bf16[128,2048]{1,0:T(8,128)(2,1)} %tok_hbm.1, bf16[128,2048]{1,0:T(8,128)(2,1)} %cot_hbm.1, s32[2,128]{1,0:T(2,128)} %bitcast.24, bf16[4,2048]{1,0:T(4,128)(2,1)} %bitcast.22, bf16[16,2048]{1,0:T(8,128)(2,1)} %bitcast.20), custom_call_target="tpu_custom_call" | custom-call | flops 134217728 | tf_op jit(solution)/shard_map/pallas_call | solution.py:48
  3.8 5.1 %collective-permute-start.1 = (bf16[64,2176]{1,0:T(8,128)(2,1)}, bf16[64,2176]{1,0:T(8,128)(2,1)S(1)}, u32[]{:S(2)}, u32[]{:S(2)}) collective-permute-start(bf16[64,2176]{1,0:T(8,128)(2,1)} %get-tuple-element.57), channel_id=1, source_target_pairs={{0,24},{1,17},{2,26},{3,19},{4,28},{5,21},{6,30},{7,23},{8,16},{9,... | collective-permute-start | bytes 835592 | tf_op jit(solution)/shard_map/ppermute | solution.py:400
  8.9 1.7 %collective-permute-start = (bf16[64,4224]{1,0:T(8,128)(2,1)}, bf16[64,4224]{1,0:T(8,128)(2,1)S(1)}, u32[]{:S(2)}, u32[]{:S(2)}) collective-permute-start(bf16[64,4224]{1,0:T(8,128)(2,1)} %get-tuple-element.56), channel_id=1, source_target_pairs={{0,0},{1,9},{2,2},{3,11},{4,4},{5,13},{6,6},{7,15},{8,8},{9,1},{10... | collective-permute-start | bytes 1622024 | tf_op jit(solution)/shard_map/ppermute | solution.py:400
  11.3 5.4 %collective-permute-done.1.meta_ref.tok_ref = bf16[64,2176]{1,0:T(8,128)(2,1)S(1)} collective-permute-done((bf16[64,2176]{1,0:T(8,128)(2,1)}, bf16[64,2176]{1,0:T(8,128)(2,1)S(1)}, u32[]{:S(2)}, u32[]{:S(2)}) %collective-permute-start.1) | collective-permute-done | bytes 278560 | tf_op jit(solution)/shard_map/ppermute | solution.py:400
  16.7 5.7 %collective-permute-start.14 = (bf16[256,2048]{1,0:T(8,128)(2,1)}, bf16[256,2048]{1,0:T(8,128)(2,1)S(1)}, u32[]{:S(2)}, u32[]{:S(2)}) collective-permute-start(bf16[256,2048]{1,0:T(8,128)(2,1)} %bitcast.18), channel_id=1, source_target_pairs={{0,1},{1,0},{2,3},{3,2},{4,5},{5,4},{6,7},{7,6},{8,9},{9,8},{10,11... | collective-permute-start | bytes 3145736 | tf_op jit(solution)/shard_map/ppermute | solution.py:409
  22.9 1.7 %collective-permute-start.10 = (bf16[32,2176]{1,0:T(8,128)(2,1)S(1)}, bf16[32,2176]{1,0:T(8,128)(2,1)S(1)}, u32[]{:S(2)}, u32[]{:S(2)}) collective-permute-start(bf16[32,2176]{1,0:T(8,128)(2,1)S(1)} %get-tuple-element.69), channel_id=1, source_target_pairs={{0,4},{2,6},{4,0},{6,2},{8,12},{10,14},{12,8},{14,10},{16,20},{18,... | collective-permute-start | bytes 417800 | tf_op jit(solution)/shard_map/ppermute | solution.py:405
  28.1 1.6 %collective-permute-start.2 = (bf16[32,4224]{1,0:T(8,128)(2,1)S(1)}, bf16[32,4224]{1,0:T(8,128)(2,1)S(1)}, u32[]{:S(2)}, u32[]{:S(2)}) collective-permute-start(bf16[32,4224]{1,0:T(8,128)(2,1)S(1)} %get-tuple-element.59), channel_id=1, source_target_pairs={{0,2},{2,0},{4,6},{6,4},{8,10},{10,8},{12,14},{14,12},{16,18},{18,... | collective-permute-start | bytes 811016 | tf_op jit(solution)/shard_map/ppermute | solution.py:405
  32.1 5.3 %collective-permute-done.9.refs_5_.refs_9_ = bf16[32,2176]{1,0:T(8,128)(2,1)S(1)} collective-permute-done((bf16[32,2176]{1,0:T(8,128)(2,1)S(1)}, bf16[32,2176]{1,0:T(8,128)(2,1)S(1)}, u32[]{:S(2)}, u32[]{:S(2)}) %collective-permute-start.9) | collective-permute-done | bytes 139296 | tf_op jit(solution)/shard_map/ppermute | solution.py:405
  37.5 4.5 %collective-permute-start.3 = (bf16[32,4224]{1,0:T(8,128)(2,1)S(1)}, bf16[32,4224]{1,0:T(8,128)(2,1)S(1)}, u32[]{:S(2)}, u32[]{:S(2)}) collective-permute-start(bf16[32,4224]{1,0:T(8,128)(2,1)S(1)} %get-tuple-element.60), channel_id=1, source_target_pairs={{0,4},{2,6},{4,0},{6,2},{8,12},{10,14},{12,8},{14,10},{16,20},{18,... | collective-permute-start | bytes 811016 | tf_op jit(solution)/shard_map/ppermute | solution.py:405
  42.3 11.3 %collective-permute-done.3.refs_2_ = bf16[32,4224]{1,0:T(8,128)(2,1)S(1)} collective-permute-done((bf16[32,4224]{1,0:T(8,128)(2,1)S(1)}, bf16[32,4224]{1,0:T(8,128)(2,1)S(1)}, u32[]{:S(2)}, u32[]{:S(2)}) %collective-permute-start.3) | collective-permute-done | bytes 270368 | tf_op jit(solution)/shard_map/ppermute | solution.py:405
  53.7 2.5 %collective-permute-start.7 = (bf16[32,2048]{1,0:T(8,128)(2,1)S(1)}, bf16[32,2048]{1,0:T(8,128)(2,1)S(1)}, u32[]{:S(2)}, u32[]{:S(2)}) collective-permute-start(bf16[32,2048]{1,0:T(8,128)(2,1)S(1)} %get-tuple-element.65), channel_id=1, source_target_pairs={{0,4},{2,6},{4,0},{6,2},{8,12},{10,14},{12,8},{14,10},{16,20},{18,... | collective-permute-start | bytes 393224 | tf_op jit(solution)/shard_map/ppermute | solution.py:405
  57.8 2.0 %shard_map.163 = (bf16[256,2048]{1,0:T(8,128)(2,1)}, f32[256,256]{1,0:T(8,128)S(1)}, f32[256,256]{1,0:T(8,128)S(1)}, f32[256,256]{1,0:T(8,128)S(1)}, f32[256,256]{1,0:T(8,128)S(1)}) custom-call(bf16[32,4224]{1,0:T(8,128)(2,1)S(1)} %get-tuple-element.58.refs_0_, bf16[32,4224]{1,0:T(8,128)(2,1)S(1)} %collective-permute-done.2.refs_1_, ...), custom_call_target="tpu_custom_call" | custom-call | flops 1073741824 | tf_op jit(solution)/shard_map/pallas_call | solution.py:48
  60.1 2.7 %collective-permute-done.7.refs_6_ = bf16[32,2048]{1,0:T(8,128)(2,1)S(1)} collective-permute-done((bf16[32,2048]{1,0:T(8,128)(2,1)S(1)}, bf16[32,2048]{1,0:T(8,128)(2,1)S(1)}, u32[]{:S(2)}, u32[]{:S(2)}) %collective-permute-start.7) | collective-permute-done | bytes 131104 | tf_op jit(solution)/shard_map/ppermute | solution.py:405
  62.7 1.9 %collective-permute-done.8.refs_7_ = bf16[32,2048]{1,0:T(8,128)(2,1)S(1)} collective-permute-done((bf16[32,2048]{1,0:T(8,128)(2,1)S(1)}, bf16[32,2048]{1,0:T(8,128)(2,1)S(1)}, u32[]{:S(2)}, u32[]{:S(2)}) %collective-permute-start.8) | collective-permute-done | bytes 131104 | tf_op jit(solution)/shard_map/ppermute | solution.py:405
  64.6 4.2 %shard_map.164 = (bf16[256,768]{1,0:T(8,128)(2,1)S(1)}, bf16[256,768]{1,0:T(8,128)(2,1)}, bf16[256,2048]{1,0:T(8,128)(2,1)S(1)}, f32[256,128]{1,0:T(8,128)S(1)},...) custom-call(bf16[32,4224]{1,0:T(8,128)(2,1)S(1)} %get-tuple-element., ...), custom_call_target="tpu_custom_call" | custom-call | flops 1610612736 | tf_op jit(solution)/shard_map/pallas_call | solution.py:48
  69.4 1.7 %collective-permute-start.16 = (bf16[64,2176]{1,0:T(8,128)(2,1)S(1)}, bf16[64,2176]{1,0:T(8,128)(2,1)S(1)}, u32[]{:S(2)}, u32[]{:S(2)}) collective-permute-start(bf16[64,2176]{1,0:T(8,128)(2,1)S(1)} %get-tuple-element.77), channel_id=1, source_target_pairs={{0,4},{2,6},{4,0},{6,2},{8,12},{10,14},{12,8},{14,10},{16,20},{18,... | collective-permute-start | bytes 835592 | tf_op jit(solution)/shard_map/ppermute | solution.py:405
  73.2 5.1 %collective-permute-done.15.refs_1_ = bf16[64,2176]{1,0:T(8,128)(2,1)S(1)} collective-permute-done((bf16[64,2176]{1,0:T(8,128)(2,1)S(1)}, bf16[64,2176]{1,0:T(8,128)(2,1)S(1)}, u32[]{:S(2)}, u32[]{:S(2)}) %collective-permute-start.15) | collective-permute-done | bytes 278560 | tf_op jit(solution)/shard_map/ppermute | solution.py:405
  78.3 5.3 %collective-permute-done.16.refs_2_ = bf16[64,2176]{1,0:T(8,128)(2,1)S(1)} collective-permute-done((bf16[64,2176]{1,0:T(8,128)(2,1)S(1)}, bf16[64,2176]{1,0:T(8,128)(2,1)S(1)}, u32[]{:S(2)}, u32[]{:S(2)}) %collective-permute-start.16) | collective-permute-done | bytes 278560 | tf_op jit(solution)/shard_map/ppermute | solution.py:405
  85.3 7.2 %collective-permute-start.19 = (bf16[64,2048]{1,0:T(8,128)(2,1)S(1)}, bf16[64,2048]{1,0:T(8,128)(2,1)S(1)}, u32[]{:S(2)}, u32[]{:S(2)}) collective-permute-start(bf16[64,2048]{1,0:T(8,128)(2,1)S(1)} %get-tuple-element.80), channel_id=1, source_target_pairs={{0,24},{1,17},{2,26},{3,19},{4,28},{5,21},{6,30},{7,23},{8,16},{9,... | collective-permute-start | bytes 786440 | tf_op jit(solution)/shard_map/ppermute | solution.py:400
  93.0 6.8 %collective-permute-done.19.y1_ref = bf16[64,2048]{1,0:T(8,128)(2,1)S(1)} collective-permute-done((bf16[64,2048]{1,0:T(8,128)(2,1)S(1)}, bf16[64,2048]{1,0:T(8,128)(2,1)S(1)}, u32[]{:S(2)}, u32[]{:S(2)}) %collective-permute-start.19) | collective-permute-done | bytes 262176 | tf_op jit(solution)/shard_map/ppermute | solution.py:400
  100.8 4.6 %collective-permute-start.20 = (bf16[128,1024]{1,0:T(8,128)(2,1)}, bf16[128,1024]{1,0:T(8,128)(2,1)S(1)}, u32[]{:S(2)}, u32[]{:S(2)}) collective-permute-start(bf16[128,1024]{1,0:T(8,128)(2,1)} %get-tuple-element.82), channel_id=1, source_target_pairs={{0,1},{1,0},{2,3},{3,2},{4,5},{5,4},{6,7},{7,6},{8,9},{9,8},{10,11... | collective-permute-start | bytes 786440 | tf_op jit(solution)/shard_map/ppermute | solution.py:409
  107.6 4.5 %all-to-all-start = ((f32[16,16,128]{2,1,0:T(8,128)}), f32[16,16,128]{2,1,0:T(8,128)S(1)}, u32[]{:S(2)}, u32[]{:S(2)}) async-start(f32[16,16,128]{2,1,0:T(8,128)} %add.3), calls=%async_computation | async-start | bytes 262144 | tf_op jit(solution)/shard_map/all_to_all | solution.py:498
  112.9 5.2 %shard_map.168 = (bf16[2048,256]{1,0:T(8,128)(2,1)}, bf16[2048,256]{1,0:T(8,128)(2,1)}, f32[2,2048]{1,0:T(2,128)S(1)}) custom-call(bf16[256,2048]{1,0:T(8,128)(2,1)} %get-tuple-element.83.x_ref, bf16[256,2048]{1,0:T(8,128)(2,1)} %collective-permute-done.21.other_ref, bf16[256,768]{1,0:T(8,128)(2,1)S(1)} %get-tuple-element.84.mine_ref, ...), custom_call_target="tpu_custom_call" | custom-call | flops 1073741824 | tf_op jit(solution)/shard_map/pallas_call | solution.py:48
  118.2 2.3 %shard_map.170 = (bf16[256,2048]{1,0:T(8,128)(2,1)}, f32[1,256]{1,0:T(1,128)}) custom-call(bf16[256,2048]{1,0:T(8,128)(2,1)S(1)} %shard_map.169.c_ref, bf16[256,2048]{1,0:T(8,128)(2,1)S(1)} %collective-permute-done.23.other_ref, bf16[256,768]{1,0:T(8,128)(2,1)S(1)} %get-tuple-element.84.mine_ref, bf16[256,768]{1,0:T(8,128)(2,1)S(1)} %collective-permute-done.22.got_ref), custom_call_target="tpu_custom_call" | custom-call | flops 536870912 | tf_op jit(solution)/shard_map/pallas_call | solution.py:48
  (59 shorter events, 18.8 us)
Async XLA Ops:
  3.8 12.9 %collective-permute-start.1 = (bf16[64,2176]{1,0:T(8,128)(2,1)}, bf16[64,2176]{1,0:T(8,128)(2,1)S(1)}, u32[]{:S(2)}, u32[]{:S(2)}) collective-permute-start(bf16[64,2176]{1,0:T(8,128)(2,1)} %get-tuple-element.57), channel_id=1, source_target_pairs={{0,24},{1,17},{2,26},{3,19},{4,28},{5,21},{6,30},{7,23},{8,16},{9,... | collective-permute-start | bytes 835592 | tf_op jit(solution)/shard_map/ppermute | solution.py:400
  8.9 15.8 %collective-permute-start = (bf16[64,4224]{1,0:T(8,128)(2,1)}, bf16[64,4224]{1,0:T(8,128)(2,1)S(1)}, u32[]{:S(2)}, u32[]{:S(2)}) collective-permute-start(bf16[64,4224]{1,0:T(8,128)(2,1)} %get-tuple-element.56), channel_id=1, source_target_pairs={{0,0},{1,9},{2,2},{3,11},{4,4},{5,13},{6,6},{7,15},{8,8},{9,1},{10... | collective-permute-start | bytes 1622024 | tf_op jit(solution)/shard_map/ppermute | solution.py:400
  10.6 45.5 %collective-permute-start.12 = (bf16[2048,256]{1,0:T(8,128)(2,1)S(1)}, bf16[2048,256]{1,0:T(8,128)(2,1)S(1)}, u32[]{:S(2)}, u32[]{:S(2)}) collective-permute-start(bf16[2048,256]{1,0:T(8,128)(2,1)S(1)} %bitcast.12), channel_id=1, source_target_pairs={{0,1},{1,0},{2,3},{3,2},{4,5},{5,4},{6,7},{7,6},{8,9},{9,8},{10,11... | collective-permute-start | bytes 3145736 | tf_op jit(solution)/shard_map/ppermute | solution.py:409
  10.7 47.0 %collective-permute-start.13 = (bf16[2048,256]{1,0:T(8,128)(2,1)}, bf16[2048,256]{1,0:T(8,128)(2,1)S(1)}, u32[]{:S(2)}, u32[]{:S(2)}) collective-permute-start(bf16[2048,256]{1,0:T(8,128)(2,1)} %bitcast.15), channel_id=1, source_target_pairs={{0,1},{1,0},{2,3},{3,2},{4,5},{5,4},{6,7},{7,6},{8,9},{9,8},{10,11... | collective-permute-start | bytes 3145736 | tf_op jit(solution)/shard_map/ppermute | solution.py:409
  11.1 11.8 %collective-permute-start.5 = (bf16[64,2048]{1,0:T(8,128)(2,1)}, bf16[64,2048]{1,0:T(8,128)(2,1)S(1)}, u32[]{:S(2)}, u32[]{:S(2)}) collective-permute-start(bf16[64,2048]{1,0:T(8,128)(2,1)} %get-tuple-element.62), channel_id=1, source_target_pairs={{0,24},{1,17},{2,26},{3,19},{4,28},{5,21},{6,30},{7,23},{8,16},{9,... | collective-permute-start | bytes 786440 | tf_op jit(solution)/shard_map/ppermute | solution.py:400
  16.7 47.9 %collective-permute-start.14 = (bf16[256,2048]{1,0:T(8,128)(2,1)}, bf16[256,2048]{1,0:T(8,128)(2,1)S(1)}, u32[]{:S(2)}, u32[]{:S(2)}) collective-permute-start(bf16[256,2048]{1,0:T(8,128)(2,1)} %bitcast.18), channel_id=1, source_target_pairs={{0,1},{1,0},{2,3},{3,2},{4,5},{5,4},{6,7},{7,6},{8,9},{9,8},{10,11... | collective-permute-start | bytes 3145736 | tf_op jit(solution)/shard_map/ppermute | solution.py:409
  24.7 6.0 %collective-permute-start.11 = (bf16[32,2176]{1,0:T(8,128)(2,1)S(1)}, bf16[32,2176]{1,0:T(8,128)(2,1)S(1)}, u32[]{:S(2)}, u32[]{:S(2)}) collective-permute-start(bf16[32,2176]{1,0:T(8,128)(2,1)S(1)} %get-tuple-element.70), channel_id=1, source_target_pairs={{0,6},{2,4},{4,2},{6,0},{8,14},{10,12},{12,10},{14,8},{16,22},{18,... | collective-permute-start | bytes 417800 | tf_op jit(solution)/shard_map/ppermute | solution.py:405
  28.1 13.9 %collective-permute-start.2 = (bf16[32,4224]{1,0:T(8,128)(2,1)S(1)}, bf16[32,4224]{1,0:T(8,128)(2,1)S(1)}, u32[]{:S(2)}, u32[]{:S(2)}) collective-permute-start(bf16[32,4224]{1,0:T(8,128)(2,1)S(1)} %get-tuple-element.59), channel_id=1, source_target_pairs={{0,2},{2,0},{4,6},{6,4},{8,10},{10,8},{12,14},{14,12},{16,18},{18,... | collective-permute-start | bytes 811016 | tf_op jit(solution)/shard_map/ppermute | solution.py:405
  30.6 6.8 %collective-permute-start.9 = (bf16[32,2176]{1,0:T(8,128)(2,1)S(1)}, bf16[32,2176]{1,0:T(8,128)(2,1)S(1)}, u32[]{:S(2)}, u32[]{:S(2)}) collective-permute-start(bf16[32,2176]{1,0:T(8,128)(2,1)S(1)} %get-tuple-element.68), channel_id=1, source_target_pairs={{0,2},{2,0},{4,6},{6,4},{8,10},{10,8},{12,14},{14,12},{16,18},{18,... | collective-permute-start | bytes 417800 | tf_op jit(solution)/shard_map/ppermute | solution.py:405
  37.5 16.2 %collective-permute-start.3 = (bf16[32,4224]{1,0:T(8,128)(2,1)S(1)}, bf16[32,4224]{1,0:T(8,128)(2,1)S(1)}, u32[]{:S(2)}, u32[]{:S(2)}) collective-permute-start(bf16[32,4224]{1,0:T(8,128)(2,1)S(1)} %get-tuple-element.60), channel_id=1, source_target_pairs={{0,4},{2,6},{4,0},{6,2},{8,12},{10,14},{12,8},{14,10},{16,20},{18,... | collective-permute-start | bytes 811016 | tf_op jit(solution)/shard_map/ppermute | solution.py:405
  42.0 11.7 %collective-permute-start.4 = (bf16[32,4224]{1,0:T(8,128)(2,1)S(1)}, bf16[32,4224]{1,0:T(8,128)(2,1)S(1)}, u32[]{:S(2)}, u32[]{:S(2)}) collective-permute-start(bf16[32,4224]{1,0:T(8,128)(2,1)S(1)} %get-tuple-element.61), channel_id=1, source_target_pairs={{0,6},{2,4},{4,2},{6,0},{8,14},{10,12},{12,10},{14,8},{16,22},{18,... | collective-permute-start | bytes 811016 | tf_op jit(solution)/shard_map/ppermute | solution.py:405
  53.7 6.4 %collective-permute-start.6 = (bf16[32,2048]{1,0:T(8,128)(2,1)S(1)}, bf16[32,2048]{1,0:T(8,128)(2,1)S(1)}, u32[]{:S(2)}, u32[]{:S(2)}) collective-permute-start(bf16[32,2048]{1,0:T(8,128)(2,1)S(1)} %get-tuple-element.64), channel_id=1, source_target_pairs={{0,2},{2,0},{4,6},{6,4},{8,10},{10,8},{12,14},{14,12},{16,18},{18,... | collective-permute-start | bytes 393224 | tf_op jit(solution)/shard_map/ppermute | solution.py:405
  53.7 9.0 %collective-permute-start.7 = (bf16[32,2048]{1,0:T(8,128)(2,1)S(1)}, bf16[32,2048]{1,0:T(8,128)(2,1)S(1)}, u32[]{:S(2)}, u32[]{:S(2)}) collective-permute-start(bf16[32,2048]{1,0:T(8,128)(2,1)S(1)} %get-tuple-element.65), channel_id=1, source_target_pairs={{0,4},{2,6},{4,0},{6,2},{8,12},{10,14},{12,8},{14,10},{16,20},{18,... | collective-permute-start | bytes 393224 | tf_op jit(solution)/shard_map/ppermute | solution.py:405
  56.1 8.5 %collective-permute-start.8 = (bf16[32,2048]{1,0:T(8,128)(2,1)S(1)}, bf16[32,2048]{1,0:T(8,128)(2,1)S(1)}, u32[]{:S(2)}, u32[]{:S(2)}) collective-permute-start(bf16[32,2048]{1,0:T(8,128)(2,1)S(1)} %get-tuple-element.66), channel_id=1, source_target_pairs={{0,6},{2,4},{4,2},{6,0},{8,14},{10,12},{12,10},{14,8},{16,22},{18,... | collective-permute-start | bytes 393224 | tf_op jit(solution)/shard_map/ppermute | solution.py:405
  59.8 53.1 %collective-permute-start.21 = (bf16[256,2048]{1,0:T(8,128)(2,1)}, bf16[256,2048]{1,0:T(8,128)(2,1)}, u32[]{:S(2)}, u32[]{:S(2)}) collective-permute-start(bf16[256,2048]{1,0:T(8,128)(2,1)} %get-tuple-element.83.x_ref), channel_id=1, source_target_pairs={{0,1},{1,0},{2,3},{3,2},{4,5},{5,4},{6,7},{7,6},{8,9},{9,8},{10,11... | collective-permute-start | bytes 3145736 | tf_op jit(solution)/shard_map/ppermute | solution.py:409
  68.8 9.5 %collective-permute-start.15 = (bf16[64,2176]{1,0:T(8,128)(2,1)S(1)}, bf16[64,2176]{1,0:T(8,128)(2,1)S(1)}, u32[]{:S(2)}, u32[]{:S(2)}) collective-permute-start(bf16[64,2176]{1,0:T(8,128)(2,1)S(1)} %get-tuple-element.76), channel_id=1, source_target_pairs={{0,2},{2,0},{4,6},{6,4},{8,10},{10,8},{12,14},{14,12},{16,18},{18,... | collective-permute-start | bytes 835592 | tf_op jit(solution)/shard_map/ppermute | solution.py:405
  69.4 14.2 %collective-permute-start.16 = (bf16[64,2176]{1,0:T(8,128)(2,1)S(1)}, bf16[64,2176]{1,0:T(8,128)(2,1)S(1)}, u32[]{:S(2)}, u32[]{:S(2)}) collective-permute-start(bf16[64,2176]{1,0:T(8,128)(2,1)S(1)} %get-tuple-element.77), channel_id=1, source_target_pairs={{0,4},{2,6},{4,0},{6,2},{8,12},{10,14},{12,8},{14,10},{16,20},{18,... | collective-permute-start | bytes 835592 | tf_op jit(solution)/shard_map/ppermute | solution.py:405
  71.2 12.5 %collective-permute-start.17 = (bf16[64,2176]{1,0:T(8,128)(2,1)S(1)}, bf16[64,2176]{1,0:T(8,128)(2,1)S(1)}, u32[]{:S(2)}, u32[]{:S(2)}) collective-permute-start(bf16[64,2176]{1,0:T(8,128)(2,1)S(1)} %get-tuple-element.78), channel_id=1, source_target_pairs={{0,6},{2,4},{4,2},{6,0},{8,14},{10,12},{12,10},{14,8},{16,22},{18,... | collective-permute-start | bytes 835592 | tf_op jit(solution)/shard_map/ppermute | solution.py:405
  72.5 45.6 %collective-permute-start.23 = (bf16[256,2048]{1,0:T(8,128)(2,1)S(1)}, bf16[256,2048]{1,0:T(8,128)(2,1)S(1)}, u32[]{:S(2)}, u32[]{:S(2)}) collective-permute-start(bf16[256,2048]{1,0:T(8,128)(2,1)S(1)} %shard_map.169.c_ref), channel_id=1, source_target_pairs={{0,1},{1,0},{2,3},{3,2},{4,5},{5,4},{6,7},{7,6},{8,9},{9,8},{10,11... | collective-permute-start | bytes 3145736 | tf_op jit(solution)/shard_map/ppermute | solution.py:409
  84.6 8.3 %collective-permute-start.18 = (bf16[64,2048]{1,0:T(8,128)(2,1)S(1)}, bf16[64,2048]{1,0:T(8,128)(2,1)S(1)}, u32[]{:S(2)}, u32[]{:S(2)}) collective-permute-start(bf16[64,2048]{1,0:T(8,128)(2,1)S(1)} %get-tuple-element.79), channel_id=1, source_target_pairs={{0,0},{1,9},{2,2},{3,11},{4,4},{5,13},{6,6},{7,15},{8,8},{9,1},{10... | collective-permute-start | bytes 786440 | tf_op jit(solution)/shard_map/ppermute | solution.py:400
  85.3 14.5 %collective-permute-start.19 = (bf16[64,2048]{1,0:T(8,128)(2,1)S(1)}, bf16[64,2048]{1,0:T(8,128)(2,1)S(1)}, u32[]{:S(2)}, u32[]{:S(2)}) collective-permute-start(bf16[64,2048]{1,0:T(8,128)(2,1)S(1)} %get-tuple-element.80), channel_id=1, source_target_pairs={{0,24},{1,17},{2,26},{3,19},{4,28},{5,21},{6,30},{7,23},{8,16},{9,... | collective-permute-start | bytes 786440 | tf_op jit(solution)/shard_map/ppermute | solution.py:400
  92.5 20.4 %collective-permute-start.22 = (bf16[256,768]{1,0:T(8,128)(2,1)}, bf16[256,768]{1,0:T(8,128)(2,1)S(1)}, u32[]{:S(2)}, u32[]{:S(2)}) collective-permute-start(bf16[256,768]{1,0:T(8,128)(2,1)} %get-tuple-element.85), channel_id=1, source_target_pairs={{0,1},{1,0},{2,3},{3,2},{4,5},{5,4},{6,7},{7,6},{8,9},{9,8},{10,11... | collective-permute-start | bytes 1179656 | tf_op jit(solution)/shard_map/ppermute | solution.py:409
  100.8 11.3 %collective-permute-start.20 = (bf16[128,1024]{1,0:T(8,128)(2,1)}, bf16[128,1024]{1,0:T(8,128)(2,1)S(1)}, u32[]{:S(2)}, u32[]{:S(2)}) collective-permute-start(bf16[128,1024]{1,0:T(8,128)(2,1)} %get-tuple-element.82), channel_id=1, source_target_pairs={{0,1},{1,0},{2,3},{3,2},{4,5},{5,4},{6,7},{7,6},{8,9},{9,8},{10,11... | collective-permute-start | bytes 786440 | tf_op jit(solution)/shard_map/ppermute | solution.py:409
  107.6 12.9 %all-to-all-start = ((f32[16,16,128]{2,1,0:T(8,128)}), f32[16,16,128]{2,1,0:T(8,128)S(1)}, u32[]{:S(2)}, u32[]{:S(2)}) async-start(f32[16,16,128]{2,1,0:T(8,128)} %add.3), calls=%async_computation | async-start | bytes 262144 | tf_op jit(solution)/shard_map/all_to_all | solution.py:498
  (9 other events, 96.8 us)

commit v3 on v2

--- a/solution.py
+++ b/solution.py
@@ -171,22 +171,27 @@
 
 def forward_kernel(width, *refs):
     first, second = refs[:width], refs[width : 2 * width]
-    weights, x_ref, outs = refs[2 * width : 2 * width + 4], refs[-5], refs[-4:]
+    weights, x_ref, outs = refs[2 * width : 2 * width + 4], refs[-7], refs[-6:]
     model = x_ref.shape[1]
     cap = first[0].shape[0]
     for k in range(width):
         x_ref[k * cap : (k + 1) * cap, :] = first[k][:, :model]
         x_ref[(width + k) * cap : (width + k + 1) * cap, :] = second[k][:, :model]
     x = x_ref[...]
-    for w, out in zip(weights, outs):
-        out[...] = dot(x, w[...])
+    for n in range(2):
+        gate_pre, up_pre = dot(x, weights[n][...]), dot(x, weights[2 + n][...])
+        hid_ref, gate_ref, up_ref = outs[3 * n : 3 * n + 3]
+        sig = 1.0 / (1.0 + jnp.exp(-gate_pre))
+        silu = gate_pre * sig
+        hid_ref[...] = (silu * up_pre).astype(BF)
+        gate_ref[...] = up_pre * sig * (1.0 + gate_pre * (1.0 - sig))
+        up_ref[...] = silu
 
 
 def delta_kernel(width, *refs):
     first, second, tok = refs[:width], refs[width : 2 * width], refs[2 * width : 3 * width]
     gates, ups, downs = refs[3 * width : 3 * width + 2], refs[3 * width + 2 : 3 * width + 4], refs[3 * width + 4 : 3 * width + 6]
-    gps, upps = refs[3 * width + 6 : 3 * width + 8], refs[3 * width + 8 : 3 * width + 10]
-    outs = refs[3 * width + 10 :]
+    pre, outs = refs[3 * width + 6 : 3 * width + 12], refs[3 * width + 12 :]
     mine_ref, other_ref, c_ref, w_ref = outs[:4]
     backs = outs[4 : 4 + width]
     model = c_ref.shape[1]
@@ -203,13 +208,11 @@
     s = None
     for n, out in enumerate((mine_ref, other_ref)):
         pulled = dot_nt(c, downs[n][...])
-        gate_pre, up_pre = gps[n][...], upps[n][...]
-        sig = 1.0 / (1.0 + jnp.exp(-gate_pre))
-        silu = gate_pre * sig
-        hid = (silu * up_pre).astype(BF)
+        hid_ref, gate_ref, up_ref = pre[3 * n : 3 * n + 3]
+        hid = hid_ref[...]
         dh = scale * pulled
-        out[:, :hidden] = (dh * up_pre * sig * (1.0 + gate_pre * (1.0 - sig))).astype(BF)
-        out[:, hidden : 2 * hidden] = (dh * silu).astype(BF)
+        out[:, :hidden] = (dh * gate_ref[...]).astype(BF)
+        out[:, hidden : 2 * hidden] = (dh * up_ref[...]).astype(BF)
         out[:, 2 * hidden :] = hid
         part = jnp.sum(pulled * hid.astype(F32), axis=1, keepdims=True)
         s = part if s is None else s + part
@@ -217,7 +220,7 @@
     for k in range(width):
         backs[k][:cap, model:] = wide[k * cap : (k + 1) * cap]
         backs[k][cap:, model:] = wide[(width + k) * cap : (width + k + 1) * cap]
-    step = 256
+    step = 1024
 
     @pl.loop(0, model // step)
     def _(i):
@@ -450,7 +453,8 @@
     downs = (down_mat, swap(down_mat))
     x_full, *pre = call(
         functools.partial(forward_kernel, width),
-        [sds((batch, model))] + [sds((batch, hidden), F32)] * 4,
+        [sds((batch, model))]
+        + [sds((batch, hidden)), sds((batch, hidden), F32), sds((batch, hidden), F32)] * 2,
         (*m_a, *m_t, *gates, *ups),
         flops=8 * flat,
     )

time: 122 us -> 120 us (0.984)
  Pallas kernels: 22 us -> 20.2 us
    pallas_call x13, Pallas kernels: 22 us -> 20.2 us  [call(): pl.pallas_call(kernel, out_shape=out_shapes, in_specs=in_specs, out_specs...]
  transfers between devices with their start and end apart: 27 -> 27, of which waited for: 11 -> 11; matrix products, arithmetic and copies ran while one was open for 1% -> 1% of each run, Pallas kernels for 15% -> 14%
where the time goes in v3:
time: 120 us; the launch traced here: 119 us
  starting transfers between devices  49.4 us (41%)
  waiting for transfers between devices  47.7 us (40%)
  Pallas kernels  20.2 us (17%)
    ppermute x12, waiting for transfers between devices, over_members(): moved.append(lax.ppermute(blocks[k], 'ep', [(i, i ^ k) for i in range(ep)]))  33.9 us
    pallas_call x13, Pallas kernels, call(): pl.pallas_call(kernel, out_shape=out_shapes, in_specs=in_specs, out_specs...  20.2 us
    ppermute x12, starting transfers between devices, over_members(): moved.append(lax.ppermute(blocks[k], 'ep', [(i, i ^ k) for i in range(ep)]))  18.4 us
    ppermute x5, starting transfers between devices, over_groups(): return lax.ppermute(x, ('ep', 'tp'), perm)  14.9 us
    ppermute x5, waiting for transfers between devices, over_groups(): return lax.ppermute(x, ('ep', 'tp'), perm)  12.2 us
    ppermute x9, starting transfers between devices, swap(): return lax.ppermute(x, 'tp', [(i, tp - 1 - i) for i in range(tp)])  11.7 us
    all_to_all x1, starting transfers between devices, body(): part = lax.all_to_all(part, 'ep', split_axis=0, concat_axis=0, tiled=True)  4.46 us
  transfers between devices with their start and end apart: 27, of which 11 were waited for; matrix products, arithmetic and copies ran while one was open for 1% of the time, Pallas kernels for 14%

profile of v3, /device:TPU:0, one launch (start us, length us, event | category | flops | bytes accessed | tf_op | source)
XLA Modules:
  0.0 119.4 jit_solution(14871907101881858368)
XLA Ops:
  0.7 3.1 %shard_map.159 = (bf16[64,4224]{1,0:T(8,128)(2,1)}, bf16[64,2176]{1,0:T(8,128)(2,1)}, bf16[64,2048]{1,0:T(8,128)(2,1)}, f32[8,128]{1,0:T(8,128)}) custom-call(bf16[128,2048]{1,0:T(8,128)(2,1)} %tok_hbm.1, bf16[128,2048]{1,0:T(8,128)(2,1)} %cot_hbm.1, s32[2,128]{1,0:T(2,128)} %bitcast.24, bf16[4,2048]{1,0:T(4,128)(2,1)} %bitcast.22, bf16[16,2048]{1,0:T(8,128)(2,1)} %bitcast.20), custom_call_target="tpu_custom_call" | custom-call | flops 134217728 | tf_op jit(solution)/shard_map/pallas_call | solution.py:48
  3.8 5.1 %collective-permute-start.1 = (bf16[64,2176]{1,0:T(8,128)(2,1)}, bf16[64,2176]{1,0:T(8,128)(2,1)S(1)}, u32[]{:S(2)}, u32[]{:S(2)}) collective-permute-start(bf16[64,2176]{1,0:T(8,128)(2,1)} %get-tuple-element.59), channel_id=1, source_target_pairs={{0,24},{1,17},{2,26},{3,19},{4,28},{5,21},{6,30},{7,23},{8,16},{9,... | collective-permute-start | bytes 835592 | tf_op jit(solution)/shard_map/ppermute | solution.py:403
  8.9 1.7 %collective-permute-start = (bf16[64,4224]{1,0:T(8,128)(2,1)}, bf16[64,4224]{1,0:T(8,128)(2,1)S(1)}, u32[]{:S(2)}, u32[]{:S(2)}) collective-permute-start(bf16[64,4224]{1,0:T(8,128)(2,1)} %get-tuple-element.58), channel_id=1, source_target_pairs={{0,0},{1,9},{2,2},{3,11},{4,4},{5,13},{6,6},{7,15},{8,8},{9,1},{10... | collective-permute-start | bytes 1622024 | tf_op jit(solution)/shard_map/ppermute | solution.py:403
  11.3 5.4 %collective-permute-done.1.meta_ref.tok_ref = bf16[64,2176]{1,0:T(8,128)(2,1)S(1)} collective-permute-done((bf16[64,2176]{1,0:T(8,128)(2,1)}, bf16[64,2176]{1,0:T(8,128)(2,1)S(1)}, u32[]{:S(2)}, u32[]{:S(2)}) %collective-permute-start.1) | collective-permute-done | bytes 278560 | tf_op jit(solution)/shard_map/ppermute | solution.py:403
  16.7 5.7 %collective-permute-start.14 = (bf16[256,2048]{1,0:T(8,128)(2,1)}, bf16[256,2048]{1,0:T(8,128)(2,1)S(1)}, u32[]{:S(2)}, u32[]{:S(2)}) collective-permute-start(bf16[256,2048]{1,0:T(8,128)(2,1)} %bitcast.18), channel_id=1, source_target_pairs={{0,1},{1,0},{2,3},{3,2},{4,5},{5,4},{6,7},{7,6},{8,9},{9,8},{10,11... | collective-permute-start | bytes 3145736 | tf_op jit(solution)/shard_map/ppermute | solution.py:412
  22.9 1.7 %collective-permute-start.10 = (bf16[32,2176]{1,0:T(8,128)(2,1)S(1)}, bf16[32,2176]{1,0:T(8,128)(2,1)S(1)}, u32[]{:S(2)}, u32[]{:S(2)}) collective-permute-start(bf16[32,2176]{1,0:T(8,128)(2,1)S(1)} %get-tuple-element.71), channel_id=1, source_target_pairs={{0,4},{2,6},{4,0},{6,2},{8,12},{10,14},{12,8},{14,10},{16,20},{18,... | collective-permute-start | bytes 417800 | tf_op jit(solution)/shard_map/ppermute | solution.py:408
  28.1 1.6 %collective-permute-start.2 = (bf16[32,4224]{1,0:T(8,128)(2,1)S(1)}, bf16[32,4224]{1,0:T(8,128)(2,1)S(1)}, u32[]{:S(2)}, u32[]{:S(2)}) collective-permute-start(bf16[32,4224]{1,0:T(8,128)(2,1)S(1)} %get-tuple-element.61), channel_id=1, source_target_pairs={{0,2},{2,0},{4,6},{6,4},{8,10},{10,8},{12,14},{14,12},{16,18},{18,... | collective-permute-start | bytes 811016 | tf_op jit(solution)/shard_map/ppermute | solution.py:408
  32.1 5.3 %collective-permute-done.9.refs_5_.refs_9_ = bf16[32,2176]{1,0:T(8,128)(2,1)S(1)} collective-permute-done((bf16[32,2176]{1,0:T(8,128)(2,1)S(1)}, bf16[32,2176]{1,0:T(8,128)(2,1)S(1)}, u32[]{:S(2)}, u32[]{:S(2)}) %collective-permute-start.9) | collective-permute-done | bytes 139296 | tf_op jit(solution)/shard_map/ppermute | solution.py:408
  37.5 4.5 %collective-permute-start.3 = (bf16[32,4224]{1,0:T(8,128)(2,1)S(1)}, bf16[32,4224]{1,0:T(8,128)(2,1)S(1)}, u32[]{:S(2)}, u32[]{:S(2)}) collective-permute-start(bf16[32,4224]{1,0:T(8,128)(2,1)S(1)} %get-tuple-element.62), channel_id=1, source_target_pairs={{0,4},{2,6},{4,0},{6,2},{8,12},{10,14},{12,8},{14,10},{16,20},{18,... | collective-permute-start | bytes 811016 | tf_op jit(solution)/shard_map/ppermute | solution.py:408
  42.3 11.3 %collective-permute-done.3.refs_2_ = bf16[32,4224]{1,0:T(8,128)(2,1)S(1)} collective-permute-done((bf16[32,4224]{1,0:T(8,128)(2,1)S(1)}, bf16[32,4224]{1,0:T(8,128)(2,1)S(1)}, u32[]{:S(2)}, u32[]{:S(2)}) %collective-permute-start.3) | collective-permute-done | bytes 270368 | tf_op jit(solution)/shard_map/ppermute | solution.py:408
  53.7 2.5 %collective-permute-start.7 = (bf16[32,2048]{1,0:T(8,128)(2,1)S(1)}, bf16[32,2048]{1,0:T(8,128)(2,1)S(1)}, u32[]{:S(2)}, u32[]{:S(2)}) collective-permute-start(bf16[32,2048]{1,0:T(8,128)(2,1)S(1)} %get-tuple-element.67), channel_id=1, source_target_pairs={{0,4},{2,6},{4,0},{6,2},{8,12},{10,14},{12,8},{14,10},{16,20},{18,... | collective-permute-start | bytes 393224 | tf_op jit(solution)/shard_map/ppermute | solution.py:408
  57.8 2.0 %shard_map.163 = (bf16[256,2048]{1,0:T(8,128)(2,1)}, bf16[256,256]{1,0:T(8,128)(2,1)S(1)}, f32[256,256]{1,0:T(8,128)S(1)}, f32[256,256]{1,0:T(8,128)S(1)}, bf16[...) custom-call(bf16[32,4224]{1,0:T(8,128)(2,1)S(1)} %get-tuple-element.60.refs_0_, ...), custom_call_target="tpu_custom_call" | custom-call | flops 1073741824 | tf_op jit(solution)/shard_map/pallas_call | solution.py:48
  60.0 2.7 %collective-permute-done.7.refs_6_ = bf16[32,2048]{1,0:T(8,128)(2,1)S(1)} collective-permute-done((bf16[32,2048]{1,0:T(8,128)(2,1)S(1)}, bf16[32,2048]{1,0:T(8,128)(2,1)S(1)}, u32[]{:S(2)}, u32[]{:S(2)}) %collective-permute-start.7) | collective-permute-done | bytes 131104 | tf_op jit(solution)/shard_map/ppermute | solution.py:408
  62.7 1.9 %collective-permute-done.8.refs_7_ = bf16[32,2048]{1,0:T(8,128)(2,1)S(1)} collective-permute-done((bf16[32,2048]{1,0:T(8,128)(2,1)S(1)}, bf16[32,2048]{1,0:T(8,128)(2,1)S(1)}, u32[]{:S(2)}, u32[]{:S(2)}) %collective-permute-start.8) | collective-permute-done | bytes 131104 | tf_op jit(solution)/shard_map/ppermute | solution.py:408
  64.6 2.4 %shard_map.164 = (bf16[256,768]{1,0:T(8,128)(2,1)S(1)}, bf16[256,768]{1,0:T(8,128)(2,1)}, bf16[256,2048]{1,0:T(8,128)(2,1)S(1)}, f32[256,128]{1,0:T(8,128)S(1)},...) custom-call(bf16[32,4224]{1,0:T(8,128)(2,1)S(1)} %get-tuple-element., ...), custom_call_target="tpu_custom_call" | custom-call | flops 1610612736 | tf_op jit(solution)/shard_map/pallas_call | solution.py:48
  67.7 1.7 %collective-permute-start.16 = (bf16[64,2176]{1,0:T(8,128)(2,1)S(1)}, bf16[64,2176]{1,0:T(8,128)(2,1)S(1)}, u32[]{:S(2)}, u32[]{:S(2)}) collective-permute-start(bf16[64,2176]{1,0:T(8,128)(2,1)S(1)} %get-tuple-element.81), channel_id=1, source_target_pairs={{0,4},{2,6},{4,0},{6,2},{8,12},{10,14},{12,8},{14,10},{16,20},{18,... | collective-permute-start | bytes 835592 | tf_op jit(solution)/shard_map/ppermute | solution.py:408
  71.5 5.1 %collective-permute-done.15.refs_1_ = bf16[64,2176]{1,0:T(8,128)(2,1)S(1)} collective-permute-done((bf16[64,2176]{1,0:T(8,128)(2,1)S(1)}, bf16[64,2176]{1,0:T(8,128)(2,1)S(1)}, u32[]{:S(2)}, u32[]{:S(2)}) %collective-permute-start.15) | collective-permute-done | bytes 278560 | tf_op jit(solution)/shard_map/ppermute | solution.py:408
  76.6 5.3 %collective-permute-done.16.refs_2_ = bf16[64,2176]{1,0:T(8,128)(2,1)S(1)} collective-permute-done((bf16[64,2176]{1,0:T(8,128)(2,1)S(1)}, bf16[64,2176]{1,0:T(8,128)(2,1)S(1)}, u32[]{:S(2)}, u32[]{:S(2)}) %collective-permute-start.16) | collective-permute-done | bytes 278560 | tf_op jit(solution)/shard_map/ppermute | solution.py:408
  83.6 7.2 %collective-permute-start.19 = (bf16[64,2048]{1,0:T(8,128)(2,1)S(1)}, bf16[64,2048]{1,0:T(8,128)(2,1)S(1)}, u32[]{:S(2)}, u32[]{:S(2)}) collective-permute-start(bf16[64,2048]{1,0:T(8,128)(2,1)S(1)} %get-tuple-element.84), channel_id=1, source_target_pairs={{0,24},{1,17},{2,26},{3,19},{4,28},{5,21},{6,30},{7,23},{8,16},{9,... | collective-permute-start | bytes 786440 | tf_op jit(solution)/shard_map/ppermute | solution.py:403
  91.2 6.8 %collective-permute-done.19.y1_ref = bf16[64,2048]{1,0:T(8,128)(2,1)S(1)} collective-permute-done((bf16[64,2048]{1,0:T(8,128)(2,1)S(1)}, bf16[64,2048]{1,0:T(8,128)(2,1)S(1)}, u32[]{:S(2)}, u32[]{:S(2)}) %collective-permute-start.19) | collective-permute-done | bytes 262176 | tf_op jit(solution)/shard_map/ppermute | solution.py:403
  99.1 4.6 %collective-permute-start.20 = (bf16[128,1024]{1,0:T(8,128)(2,1)}, bf16[128,1024]{1,0:T(8,128)(2,1)S(1)}, u32[]{:S(2)}, u32[]{:S(2)}) collective-permute-start(bf16[128,1024]{1,0:T(8,128)(2,1)} %get-tuple-element.86), channel_id=1, source_target_pairs={{0,1},{1,0},{2,3},{3,2},{4,5},{5,4},{6,7},{7,6},{8,9},{9,8},{10,11... | collective-permute-start | bytes 786440 | tf_op jit(solution)/shard_map/ppermute | solution.py:412
  105.9 4.5 %all-to-all-start = ((f32[16,16,128]{2,1,0:T(8,128)}), f32[16,16,128]{2,1,0:T(8,128)S(1)}, u32[]{:S(2)}, u32[]{:S(2)}) async-start(f32[16,16,128]{2,1,0:T(8,128)} %add.3), calls=%async_computation | async-start | bytes 262144 | tf_op jit(solution)/shard_map/all_to_all | solution.py:502
  111.2 5.2 %shard_map.168 = (bf16[2048,256]{1,0:T(8,128)(2,1)}, bf16[2048,256]{1,0:T(8,128)(2,1)}, f32[2,2048]{1,0:T(2,128)S(1)}) custom-call(bf16[256,2048]{1,0:T(8,128)(2,1)} %get-tuple-element.87.x_ref, bf16[256,2048]{1,0:T(8,128)(2,1)} %collective-permute-done.21.other_ref, bf16[256,768]{1,0:T(8,128)(2,1)S(1)} %get-tuple-element.88.mine_ref, ...), custom_call_target="tpu_custom_call" | custom-call | flops 1073741824 | tf_op jit(solution)/shard_map/pallas_call | solution.py:48
  116.4 2.3 %shard_map.170 = (bf16[256,2048]{1,0:T(8,128)(2,1)}, f32[1,256]{1,0:T(1,128)}) custom-call(bf16[256,2048]{1,0:T(8,128)(2,1)S(1)} %shard_map.169.c_ref, bf16[256,2048]{1,0:T(8,128)(2,1)S(1)} %collective-permute-done.23.other_ref, bf16[256,768]{1,0:T(8,128)(2,1)S(1)} %get-tuple-element.88.mine_ref, bf16[256,768]{1,0:T(8,128)(2,1)S(1)} %collective-permute-done.22.got_ref), custom_call_target="tpu_custom_call" | custom-call | flops 536870912 | tf_op jit(solution)/shard_map/pallas_call | solution.py:48
  (59 shorter events, 18.8 us)
Async XLA Ops:
  3.8 12.9 %collective-permute-start.1 = (bf16[64,2176]{1,0:T(8,128)(2,1)}, bf16[64,2176]{1,0:T(8,128)(2,1)S(1)}, u32[]{:S(2)}, u32[]{:S(2)}) collective-permute-start(bf16[64,2176]{1,0:T(8,128)(2,1)} %get-tuple-element.59), channel_id=1, source_target_pairs={{0,24},{1,17},{2,26},{3,19},{4,28},{5,21},{6,30},{7,23},{8,16},{9,... | collective-permute-start | bytes 835592 | tf_op jit(solution)/shard_map/ppermute | solution.py:403
  8.9 15.8 %collective-permute-start = (bf16[64,4224]{1,0:T(8,128)(2,1)}, bf16[64,4224]{1,0:T(8,128)(2,1)S(1)}, u32[]{:S(2)}, u32[]{:S(2)}) collective-permute-start(bf16[64,4224]{1,0:T(8,128)(2,1)} %get-tuple-element.58), channel_id=1, source_target_pairs={{0,0},{1,9},{2,2},{3,11},{4,4},{5,13},{6,6},{7,15},{8,8},{9,1},{10... | collective-permute-start | bytes 1622024 | tf_op jit(solution)/shard_map/ppermute | solution.py:403
  10.6 45.5 %collective-permute-start.12 = (bf16[2048,256]{1,0:T(8,128)(2,1)S(1)}, bf16[2048,256]{1,0:T(8,128)(2,1)S(1)}, u32[]{:S(2)}, u32[]{:S(2)}) collective-permute-start(bf16[2048,256]{1,0:T(8,128)(2,1)S(1)} %bitcast.12), channel_id=1, source_target_pairs={{0,1},{1,0},{2,3},{3,2},{4,5},{5,4},{6,7},{7,6},{8,9},{9,8},{10,11... | collective-permute-start | bytes 3145736 | tf_op jit(solution)/shard_map/ppermute | solution.py:412
  10.7 47.0 %collective-permute-start.13 = (bf16[2048,256]{1,0:T(8,128)(2,1)}, bf16[2048,256]{1,0:T(8,128)(2,1)S(1)}, u32[]{:S(2)}, u32[]{:S(2)}) collective-permute-start(bf16[2048,256]{1,0:T(8,128)(2,1)} %bitcast.15), channel_id=1, source_target_pairs={{0,1},{1,0},{2,3},{3,2},{4,5},{5,4},{6,7},{7,6},{8,9},{9,8},{10,11... | collective-permute-start | bytes 3145736 | tf_op jit(solution)/shard_map/ppermute | solution.py:412
  11.1 11.8 %collective-permute-start.5 = (bf16[64,2048]{1,0:T(8,128)(2,1)}, bf16[64,2048]{1,0:T(8,128)(2,1)S(1)}, u32[]{:S(2)}, u32[]{:S(2)}) collective-permute-start(bf16[64,2048]{1,0:T(8,128)(2,1)} %get-tuple-element.64), channel_id=1, source_target_pairs={{0,24},{1,17},{2,26},{3,19},{4,28},{5,21},{6,30},{7,23},{8,16},{9,... | collective-permute-start | bytes 786440 | tf_op jit(solution)/shard_map/ppermute | solution.py:403
  16.7 47.9 %collective-permute-start.14 = (bf16[256,2048]{1,0:T(8,128)(2,1)}, bf16[256,2048]{1,0:T(8,128)(2,1)S(1)}, u32[]{:S(2)}, u32[]{:S(2)}) collective-permute-start(bf16[256,2048]{1,0:T(8,128)(2,1)} %bitcast.18), channel_id=1, source_target_pairs={{0,1},{1,0},{2,3},{3,2},{4,5},{5,4},{6,7},{7,6},{8,9},{9,8},{10,11... | collective-permute-start | bytes 3145736 | tf_op jit(solution)/shard_map/ppermute | solution.py:412
  24.7 6.0 %collective-permute-start.11 = (bf16[32,2176]{1,0:T(8,128)(2,1)S(1)}, bf16[32,2176]{1,0:T(8,128)(2,1)S(1)}, u32[]{:S(2)}, u32[]{:S(2)}) collective-permute-start(bf16[32,2176]{1,0:T(8,128)(2,1)S(1)} %get-tuple-element.72), channel_id=1, source_target_pairs={{0,6},{2,4},{4,2},{6,0},{8,14},{10,12},{12,10},{14,8},{16,22},{18,... | collective-permute-start | bytes 417800 | tf_op jit(solution)/shard_map/ppermute | solution.py:408
  28.1 13.9 %collective-permute-start.2 = (bf16[32,4224]{1,0:T(8,128)(2,1)S(1)}, bf16[32,4224]{1,0:T(8,128)(2,1)S(1)}, u32[]{:S(2)}, u32[]{:S(2)}) collective-permute-start(bf16[32,4224]{1,0:T(8,128)(2,1)S(1)} %get-tuple-element.61), channel_id=1, source_target_pairs={{0,2},{2,0},{4,6},{6,4},{8,10},{10,8},{12,14},{14,12},{16,18},{18,... | collective-permute-start | bytes 811016 | tf_op jit(solution)/shard_map/ppermute | solution.py:408
  30.6 6.8 %collective-permute-start.9 = (bf16[32,2176]{1,0:T(8,128)(2,1)S(1)}, bf16[32,2176]{1,0:T(8,128)(2,1)S(1)}, u32[]{:S(2)}, u32[]{:S(2)}) collective-permute-start(bf16[32,2176]{1,0:T(8,128)(2,1)S(1)} %get-tuple-element.70), channel_id=1, source_target_pairs={{0,2},{2,0},{4,6},{6,4},{8,10},{10,8},{12,14},{14,12},{16,18},{18,... | collective-permute-start | bytes 417800 | tf_op jit(solution)/shard_map/ppermute | solution.py:408
  37.5 16.2 %collective-permute-start.3 = (bf16[32,4224]{1,0:T(8,128)(2,1)S(1)}, bf16[32,4224]{1,0:T(8,128)(2,1)S(1)}, u32[]{:S(2)}, u32[]{:S(2)}) collective-permute-start(bf16[32,4224]{1,0:T(8,128)(2,1)S(1)} %get-tuple-element.62), channel_id=1, source_target_pairs={{0,4},{2,6},{4,0},{6,2},{8,12},{10,14},{12,8},{14,10},{16,20},{18,... | collective-permute-start | bytes 811016 | tf_op jit(solution)/shard_map/ppermute | solution.py:408
  42.0 11.7 %collective-permute-start.4 = (bf16[32,4224]{1,0:T(8,128)(2,1)S(1)}, bf16[32,4224]{1,0:T(8,128)(2,1)S(1)}, u32[]{:S(2)}, u32[]{:S(2)}) collective-permute-start(bf16[32,4224]{1,0:T(8,128)(2,1)S(1)} %get-tuple-element.63), channel_id=1, source_target_pairs={{0,6},{2,4},{4,2},{6,0},{8,14},{10,12},{12,10},{14,8},{16,22},{18,... | collective-permute-start | bytes 811016 | tf_op jit(solution)/shard_map/ppermute | solution.py:408
  53.7 6.4 %collective-permute-start.6 = (bf16[32,2048]{1,0:T(8,128)(2,1)S(1)}, bf16[32,2048]{1,0:T(8,128)(2,1)S(1)}, u32[]{:S(2)}, u32[]{:S(2)}) collective-permute-start(bf16[32,2048]{1,0:T(8,128)(2,1)S(1)} %get-tuple-element.66), channel_id=1, source_target_pairs={{0,2},{2,0},{4,6},{6,4},{8,10},{10,8},{12,14},{14,12},{16,18},{18,... | collective-permute-start | bytes 393224 | tf_op jit(solution)/shard_map/ppermute | solution.py:408
  53.7 9.0 %collective-permute-start.7 = (bf16[32,2048]{1,0:T(8,128)(2,1)S(1)}, bf16[32,2048]{1,0:T(8,128)(2,1)S(1)}, u32[]{:S(2)}, u32[]{:S(2)}) collective-permute-start(bf16[32,2048]{1,0:T(8,128)(2,1)S(1)} %get-tuple-element.67), channel_id=1, source_target_pairs={{0,4},{2,6},{4,0},{6,2},{8,12},{10,14},{12,8},{14,10},{16,20},{18,... | collective-permute-start | bytes 393224 | tf_op jit(solution)/shard_map/ppermute | solution.py:408
  56.1 8.5 %collective-permute-start.8 = (bf16[32,2048]{1,0:T(8,128)(2,1)S(1)}, bf16[32,2048]{1,0:T(8,128)(2,1)S(1)}, u32[]{:S(2)}, u32[]{:S(2)}) collective-permute-start(bf16[32,2048]{1,0:T(8,128)(2,1)S(1)} %get-tuple-element.68), channel_id=1, source_target_pairs={{0,6},{2,4},{4,2},{6,0},{8,14},{10,12},{12,10},{14,8},{16,22},{18,... | collective-permute-start | bytes 393224 | tf_op jit(solution)/shard_map/ppermute | solution.py:408
  59.8 51.4 %collective-permute-start.21 = (bf16[256,2048]{1,0:T(8,128)(2,1)}, bf16[256,2048]{1,0:T(8,128)(2,1)}, u32[]{:S(2)}, u32[]{:S(2)}) collective-permute-start(bf16[256,2048]{1,0:T(8,128)(2,1)} %get-tuple-element.87.x_ref), channel_id=1, source_target_pairs={{0,1},{1,0},{2,3},{3,2},{4,5},{5,4},{6,7},{7,6},{8,9},{9,8},{10,11... | collective-permute-start | bytes 3145736 | tf_op jit(solution)/shard_map/ppermute | solution.py:412
  67.0 9.6 %collective-permute-start.15 = (bf16[64,2176]{1,0:T(8,128)(2,1)S(1)}, bf16[64,2176]{1,0:T(8,128)(2,1)S(1)}, u32[]{:S(2)}, u32[]{:S(2)}) collective-permute-start(bf16[64,2176]{1,0:T(8,128)(2,1)S(1)} %get-tuple-element.80), channel_id=1, source_target_pairs={{0,2},{2,0},{4,6},{6,4},{8,10},{10,8},{12,14},{14,12},{16,18},{18,... | collective-permute-start | bytes 835592 | tf_op jit(solution)/shard_map/ppermute | solution.py:408
  67.7 14.2 %collective-permute-start.16 = (bf16[64,2176]{1,0:T(8,128)(2,1)S(1)}, bf16[64,2176]{1,0:T(8,128)(2,1)S(1)}, u32[]{:S(2)}, u32[]{:S(2)}) collective-permute-start(bf16[64,2176]{1,0:T(8,128)(2,1)S(1)} %get-tuple-element.81), channel_id=1, source_target_pairs={{0,4},{2,6},{4,0},{6,2},{8,12},{10,14},{12,8},{14,10},{16,20},{18,... | collective-permute-start | bytes 835592 | tf_op jit(solution)/shard_map/ppermute | solution.py:408
  69.4 12.5 %collective-permute-start.17 = (bf16[64,2176]{1,0:T(8,128)(2,1)S(1)}, bf16[64,2176]{1,0:T(8,128)(2,1)S(1)}, u32[]{:S(2)}, u32[]{:S(2)}) collective-permute-start(bf16[64,2176]{1,0:T(8,128)(2,1)S(1)} %get-tuple-element.82), channel_id=1, source_target_pairs={{0,6},{2,4},{4,2},{6,0},{8,14},{10,12},{12,10},{14,8},{16,22},{18,... | collective-permute-start | bytes 835592 | tf_op jit(solution)/shard_map/ppermute | solution.py:408
  70.8 45.6 %collective-permute-start.23 = (bf16[256,2048]{1,0:T(8,128)(2,1)S(1)}, bf16[256,2048]{1,0:T(8,128)(2,1)S(1)}, u32[]{:S(2)}, u32[]{:S(2)}) collective-permute-start(bf16[256,2048]{1,0:T(8,128)(2,1)S(1)} %shard_map.169.c_ref), channel_id=1, source_target_pairs={{0,1},{1,0},{2,3},{3,2},{4,5},{5,4},{6,7},{7,6},{8,9},{9,8},{10,11... | collective-permute-start | bytes 3145736 | tf_op jit(solution)/shard_map/ppermute | solution.py:412
  82.9 8.3 %collective-permute-start.18 = (bf16[64,2048]{1,0:T(8,128)(2,1)S(1)}, bf16[64,2048]{1,0:T(8,128)(2,1)S(1)}, u32[]{:S(2)}, u32[]{:S(2)}) collective-permute-start(bf16[64,2048]{1,0:T(8,128)(2,1)S(1)} %get-tuple-element.83), channel_id=1, source_target_pairs={{0,0},{1,9},{2,2},{3,11},{4,4},{5,13},{6,6},{7,15},{8,8},{9,1},{10... | collective-permute-start | bytes 786440 | tf_op jit(solution)/shard_map/ppermute | solution.py:403
  83.6 14.5 %collective-permute-start.19 = (bf16[64,2048]{1,0:T(8,128)(2,1)S(1)}, bf16[64,2048]{1,0:T(8,128)(2,1)S(1)}, u32[]{:S(2)}, u32[]{:S(2)}) collective-permute-start(bf16[64,2048]{1,0:T(8,128)(2,1)S(1)} %get-tuple-element.84), channel_id=1, source_target_pairs={{0,24},{1,17},{2,26},{3,19},{4,28},{5,21},{6,30},{7,23},{8,16},{9,... | collective-permute-start | bytes 786440 | tf_op jit(solution)/shard_map/ppermute | solution.py:403
  90.8 20.4 %collective-permute-start.22 = (bf16[256,768]{1,0:T(8,128)(2,1)}, bf16[256,768]{1,0:T(8,128)(2,1)S(1)}, u32[]{:S(2)}, u32[]{:S(2)}) collective-permute-start(bf16[256,768]{1,0:T(8,128)(2,1)} %get-tuple-element.89), channel_id=1, source_target_pairs={{0,1},{1,0},{2,3},{3,2},{4,5},{5,4},{6,7},{7,6},{8,9},{9,8},{10,11... | collective-permute-start | bytes 1179656 | tf_op jit(solution)/shard_map/ppermute | solution.py:412
  99.1 11.3 %collective-permute-start.20 = (bf16[128,1024]{1,0:T(8,128)(2,1)}, bf16[128,1024]{1,0:T(8,128)(2,1)S(1)}, u32[]{:S(2)}, u32[]{:S(2)}) collective-permute-start(bf16[128,1024]{1,0:T(8,128)(2,1)} %get-tuple-element.86), channel_id=1, source_target_pairs={{0,1},{1,0},{2,3},{3,2},{4,5},{5,4},{6,7},{7,6},{8,9},{9,8},{10,11... | collective-permute-start | bytes 786440 | tf_op jit(solution)/shard_map/ppermute | solution.py:412
  105.9 12.9 %all-to-all-start = ((f32[16,16,128]{2,1,0:T(8,128)}), f32[16,16,128]{2,1,0:T(8,128)S(1)}, u32[]{:S(2)}, u32[]{:S(2)}) async-start(f32[16,16,128]{2,1,0:T(8,128)} %add.3), calls=%async_computation | async-start | bytes 262144 | tf_op jit(solution)/shard_map/all_to_all | solution.py:502
  (9 other events, 96.8 us)
